TPU v7x, 32 devices: a whole 2x2x4 slice. The times are simulated.
32 devices in a mesh: sp: 4 (over y, x), tp: 8 (over z, core).
Axes of the slice: x: 2, y: 2, z: 4, core: 2. Of those that a mesh axis runs over, the one named last changes fastest.
Arguments:
- lru_input: bfloat16 [1024, 2048], P('sp', 'tp'), may hold values from -27 to 27
- gate_input: bfloat16 [1024, 2048], P('sp', 'tp'), may hold values from -6 to 6
- documents: int32 [1024], P('sp'), may hold values from 0 to 1, never falling along the last dimension, each value on 1 to 768 neighbouring positions
- conv_taps: bfloat16 [4, 2048], P(None, 'tp'), may hold values from -3 to 3
- rate_weight: bfloat16 [16, 128, 128], P('tp'), may hold values from -0.5 to 0.5
- inlet_weight: bfloat16 [16, 128, 128], P('tp'), may hold values from -0.5 to 0.5
- decay_param: float32 [2048], P('tp')
- lru_gain: float32 [2048], P('tp'), may hold values from 0.1 to 1.9
- out_weight: bfloat16 [2048, 2048], P('tp'), may hold values from -0.125 to 0.125
- residual: bfloat16 [1024, 2048], P('sp'), may hold values from -6 to 6
- ffn_gain: float32 [2048], replicated, may hold values from 0.1 to 1.9
- routes: int32 [1024, 2], P('sp'), may hold values from 0 to 3, all different within a row; in each aligned block of 32 rows (0 to 31, 32 to 63, ...) at most 32 rows name the same one
- route_weights: float32 [1024, 2], P('sp'), may hold values from 0.1 to 0.9
- w_gate: bfloat16 [4, 2048, 6144], P('sp', None, 'tp'), may hold values from -0.125 to 0.125
- w_up: bfloat16 [4, 2048, 6144], P('sp', None, 'tp'), may hold values from -0.125 to 0.125
- w_down: bfloat16 [4, 6144, 2048], P('sp', 'tp'), may hold values from -0.078125 to 0.078125
Outputs:
- mixed_out: bfloat16 [1024, 2048], P(('sp', 'tp'))
Inputs may be any that keep to these rules, and one draw needn't show every extreme that they name: `documents`: document numbers start at 0 and never fall along the sequence; a document spans at most 768 positions. `routes`: each row names 2 different experts. In each aligned block of 32 rows no expert is named by more than 32 rows, a bound that some block reaches.
All inputs are finite; a program needn't handle non-finite values.
Results may differ from a plain program's by a relative error of at most 0.017.
Values may be sent and summed in bfloat16 or wider, within the bound.
No kernel may reach another device: no remote copies, remote signals or barrier semaphores. Data moves between devices by JAX's collectives and lax.ppermute only.
A program may use at most 64 MiB of HBM per device.

v0:
```python
import functools

import jax
import jax.numpy as jnp
from jax import lax
from jax.experimental import pallas as pl
from jax.experimental.pallas import tpu as pltpu
from jax.sharding import PartitionSpec as P


EPSILON = 1e-06
RATE_SCALE = 8.0
LANES = 128
SUBLANES = 8
CORES = 2
PLANE = 4


F32 = jnp.float32
BF16 = jnp.bfloat16


def vmem_call(kernel, outs, args, scratch=(), limit_mib=4, far_args=()):
    near, far = (pl.BlockSpec(memory_space=space) for space in (pltpu.VMEM, pltpu.HBM))
    return pl.pallas_call(
        kernel,
        in_specs=[far] * len(far_args) + [near] * len(args),
        out_specs=[near] * len(outs),
        out_shape=[jax.ShapeDtypeStruct(shape, dtype) for shape, dtype in outs],
        scratch_shapes=[
            pltpu.VMEM(*what) if isinstance(what, tuple) else what for what in scratch
        ],
        compiler_params=pltpu.CompilerParams(vmem_limit_bytes=limit_mib << 20),
    )(
        *[pltpu.with_memory_space_constraint(arg, pltpu.HBM) for arg in far_args],
        *[pltpu.with_memory_space_constraint(arg, pltpu.VMEM) for arg in args],
    )


def place():
    tp_here = lax.axis_index("tp")
    return lax.axis_index("sp"), tp_here // CORES, tp_here % CORES


def flip(value, axis, distance):
    return lax.ppermute(value, axis, [(i, i ^ distance) for i in range(lax.axis_size(axis))])


def flip_plane(value, order):
    tp_count = lax.axis_size("tp")
    pairs = [
        (shard * tp_count + at, (shard ^ plane_flip(at % CORES, order)) * tp_count + at)
        for shard in range(PLANE)
        for at in range(tp_count)
    ]
    return lax.ppermute(value, ("sp", "tp"), pairs)


def plane_flip(core, order):
    return 1 + core if order == 0 else 2 - core


def flip_z(value, distance):
    return flip(value, "tp", distance * CORES)


def column(row):
    return jnp.transpose(jnp.broadcast_to(row, (LANES, row.shape[1])))


def one_minus_exp(value):
    series = jnp.ones_like(value)
    for order in range(7, 1, -1):
        series = 1.0 + value * series * (1.0 / order)
    return jnp.where(value > -0.35, -value * series, 1.0 - jnp.exp(value))


def scan_rows(decay, drive):
    rows = decay.shape[0]
    row_ids = lax.broadcasted_iota(jnp.int32, decay.shape, 0)
    distance = 1
    while distance < rows:
        if distance < SUBLANES:
            head = row_ids < distance
            earlier_decay = jnp.where(head, 1.0, pltpu.roll(decay, distance, 0))
            earlier_drive = jnp.where(head, 0.0, pltpu.roll(drive, distance, 0))
            drive = drive + decay * earlier_drive
            decay = decay * earlier_decay
        else:
            late_drive = drive[distance:] + decay[distance:] * drive[: rows - distance]
            late_decay = decay[distance:] * decay[: rows - distance]
            drive = jnp.concatenate([drive[:distance], late_drive], axis=0)
            decay = jnp.concatenate([decay[:distance], late_decay], axis=0)
        distance *= 2
    return decay, drive


def gated_terms(conv, starts, rate_w, inlet_w, decay_in):
    conv = conv.astype(BF16)
    rate = jax.nn.sigmoid(jnp.dot(conv, rate_w, preferred_element_type=F32))
    inlet = jax.nn.sigmoid(jnp.dot(conv, inlet_w, preferred_element_type=F32))
    negated = -decay_in
    soft = jnp.maximum(negated, 0.0) + jnp.log1p(jnp.exp(-jnp.abs(negated)))
    log_decay = -RATE_SCALE * rate * soft
    decay = jnp.where(starts, 0.0, jnp.exp(log_decay))
    norm = jnp.where(starts, 1.0, jnp.sqrt(one_minus_exp(2.0 * log_decay)))
    return decay, norm * inlet * conv.astype(F32)


def convolve(padded, docs, taps, at, count, lanes):
    reach = taps.shape[0] - 1
    own_doc = docs[at : at + count]
    conv = jnp.zeros((count, LANES), F32)
    for tap in range(reach + 1):
        source = slice(at - reach + tap, at - reach + tap + count)
        rows = padded[source, lanes]
        if tap < reach:
            rows = jnp.where(docs[source] == own_doc, rows, 0.0)
        conv = conv + rows * taps[tap : tap + 1, lanes].astype(F32)
    return conv, docs[at - 1 : at - 1 + count] != own_doc


EDGE = slice(SUBLANES, 2 * SUBLANES)
EDGE_DOCS = slice(2 * SUBLANES, 3 * SUBLANES)
MESSAGE_ROWS = 3 * SUBLANES


def lru_kernel(*refs):
    far, refs = refs[:13], refs[13:]
    (state_out, run_out, mix_out), refs = refs[:3], refs[3:]
    messages, refs = refs[:PLANE], refs[PLANE:]
    (taps, rate_w, inlet_w, decay_in, out_w, residual, down_w), refs = refs[:7], refs[7:]
    rows_in, gate_in, docs, gain, routes, route_w, padded, doc_cols, sems = refs
    block = residual.shape[0]
    own = pl.ds(pl.multiple_of(lax.axis_index("tp") * block, block), block)
    sources = [*far[:11], far[11].at[own], far[12]]
    targets = (
        rows_in, docs, taps, rate_w, inlet_w, decay_in, gate_in, gain, routes, route_w, out_w, residual,
        down_w,
    )
    copies = [
        pltpu.make_async_copy(source, target, sems.at[i])
        for i, (source, target) in enumerate(zip(sources, targets))
    ]
    for copy in copies:
        copy.start()
    for copy in copies[:-3]:
        copy.wait()
    positions, channels = rows_in.shape
    reach = taps.shape[0] - 1
    padded[0:SUBLANES] = jnp.zeros((SUBLANES, channels), F32)
    padded[SUBLANES:] = rows_in[...].astype(F32)
    doc_cols[0:SUBLANES] = jnp.zeros((SUBLANES, LANES), F32)
    doc_cols[SUBLANES:] = column(docs[...].astype(F32) + 1.0)
    later = lax.broadcasted_iota(jnp.int32, (positions, LANES), 0) >= reach
    for group in range(channels // LANES):
        lanes = slice(group * LANES, (group + 1) * LANES)
        conv, starts = convolve(padded, doc_cols, taps, SUBLANES, positions, lanes)
        decay, drive = gated_terms(
            conv, starts, rate_w[group], inlet_w[group], decay_in[0:1, lanes]
        )
        run, state = scan_rows(jnp.where(later, decay, 1.0), jnp.where(later, drive, 0.0))
        state_out[:, lanes] = state
        run_out[:, lanes] = run
        for message in messages:
            message[0:1, lanes] = run[positions - 1 :]
            message[1:2, lanes] = state[positions - 1 :]
        mix_out[:, lanes] = jax.nn.gelu(gate_in[:, lanes].astype(F32)) * gain[0:1, lanes]

    def ends(rows):
        begin, end = rows[SUBLANES : 2 * SUBLANES], rows[positions : positions + SUBLANES]
        row_ids = lax.broadcasted_iota(jnp.int32, begin.shape, 0)
        return jnp.where(row_ids < reach, begin, end)

    shard, _, _ = place()
    for k, message in enumerate(messages):
        dense = jnp.zeros((1, positions), F32)
        for choice in range(routes.shape[0]):
            chosen = routes[choice : choice + 1] == (shard ^ k)
            dense = dense + jnp.where(chosen, route_w[choice : choice + 1], 0.0)
        message[2:3, 0:positions] = dense
        message[EDGE, 0:channels] = ends(padded)
        message[EDGE_DOCS, 0:LANES] = ends(doc_cols)
    for copy in copies[-3:]:
        copy.wait()


def split_sum(total):
    lane_ids = lax.broadcasted_iota(jnp.int32, (total.shape[0], LANES), 1)
    high = total.astype(BF16).astype(F32)
    low = (total - high).astype(BF16).astype(F32)
    return jnp.where(lane_ids == 0, high, jnp.where(lane_ids == 1, low, 0.0)).astype(BF16)


def joined_sum(lanes):
    lanes = lanes.astype(F32)
    return lanes[:, 0:1] + lanes[:, 1:2]


def mix_kernel(state, run, mix, taps, rate_w, inlet_w, decay_in, *rest, block):
    *messages, keep, send, stacked, edge, edge_docs, terms, heads, hidden, mixed = rest
    channels = state.shape[1]
    reach = taps.shape[0] - 1
    for k, message in enumerate(messages):
        stacked[k] = message[...]
    shard, _, core = place()
    pair = 2 * SUBLANES
    for j in range(PLANE):
        here = stacked.at[j ^ shard]
        at = j * pair
        if j == 0:
            edge[at : at + SUBLANES] = jnp.zeros((SUBLANES, channels), F32)
            edge_docs[at : at + SUBLANES] = jnp.zeros((SUBLANES, LANES), F32)
        else:
            before = stacked.at[(j - 1) ^ shard]
            edge[at : at + SUBLANES] = before[EDGE, :channels]
            edge_docs[at : at + SUBLANES] = before[EDGE_DOCS, :LANES]
        edge[at + SUBLANES : at + pair] = here[EDGE, :channels]
        edge_docs[at + SUBLANES : at + pair] = here[EDGE_DOCS, :LANES]
    for group in range(channels // LANES):
        lanes = slice(group * LANES, (group + 1) * LANES)
        firsts = [
            convolve(edge, edge_docs, taps, j * pair + SUBLANES, SUBLANES, lanes)
            for j in range(PLANE)
        ]
        conv = jnp.concatenate([first[0] for first in firsts], axis=0)
        for j, (_, starts) in enumerate(firsts):
            rows = slice(j * SUBLANES, (j + 1) * SUBLANES)
            heads[j, :, lanes] = jnp.where(starts, 1.0, 0.0)
        starts = jnp.concatenate([heads[j, :, lanes] for j in range(PLANE)], axis=0) > 0.5
        terms[0, :, lanes], terms[1, :, lanes] = gated_terms(
            conv, starts, rate_w[group], inlet_w[group], decay_in[0:1, lanes]
        )
    carried = jnp.zeros((1, channels), F32)
    for j in range(PLANE):
        for row in range(reach):
            at = j * SUBLANES + row
            carried = terms[0, at : at + 1] * carried + terms[1, at : at + 1]
            heads[j, row : row + 1] = carried
        here = stacked.at[j ^ shard]
        carried = here[0:1, :channels] * carried + here[1:2, :channels]
    head = heads[shard]
    hidden[...] = state[...] + run[...] * head[reach - 1 : reach]
    early = lax.broadcasted_iota(jnp.int32, (SUBLANES, channels), 0) < reach
    hidden[0:SUBLANES] = jnp.where(early, head, hidden[0:SUBLANES])
    whole = hidden[...]
    mixed[:, :channels] = (whole * mix[...]).astype(BF16)
    mixed[:, channels:] = split_sum(jnp.sum(whole * whole, axis=1, keepdims=True))
    for z in range(keep.shape[0] // block):
        rows = slice(z * block, (z + 1) * block)
        keep[rows] = mixed[pl.ds(pl.multiple_of((CORES * z + core) * block, block), block)]
        send[rows] = mixed[pl.ds(pl.multiple_of((CORES * z + 1 - core) * block, block), block)]


def project_kernel(keep, other, own_w, other_w, *rest, block):
    *outs, own_rows, other_rows = rest
    channels, width = own_w.shape
    _, depth, _ = place()
    for k in range(len(outs)):
        rows = slice(k * block, (k + 1) * block)
        source = pl.ds(pl.multiple_of((depth ^ k) * block, block), block)
        own_rows[rows] = keep[source]
        other_rows[rows] = other[source]
    squares = split_sum(joined_sum(own_rows[:, channels:]) + joined_sum(other_rows[:, channels:]))
    product = jnp.dot(own_rows[:, :channels], own_w[...], preferred_element_type=F32)
    product = product + jnp.dot(other_rows[:, :channels], other_w[...], preferred_element_type=F32)
    for k, out in enumerate(outs):
        rows = slice(k * block, (k + 1) * block)
        out[:, :width] = product[rows].astype(BF16)
        out[:, width:] = squares[rows]


def add_kernel(one, two, out):
    width = out.shape[1] - LANES
    out[:, :width] = (one[:, :width].astype(F32) + two[:, :width].astype(F32)).astype(BF16)
    out[:, width:] = split_sum(joined_sum(one[:, width:]) + joined_sum(two[:, width:]))


def norm_kernel(residual, gain, *rest, channels_total):
    *parts, after_out, normed_out = rest
    width = residual.shape[1]
    total = sum(part[:, :width].astype(F32) for part in parts)
    squares = sum(joined_sum(part[:, width:]) for part in parts)
    projected = total * lax.rsqrt(squares / channels_total + EPSILON)
    after = (residual[...].astype(F32) + projected).astype(BF16)
    after_out[...] = after
    floated = after.astype(F32)
    inverse_rms = lax.rsqrt(jnp.mean(floated * floated, axis=1, keepdims=True) + EPSILON)
    normed_out[...] = (floated * inverse_rms * gain[...]).astype(BF16)


def expert_kernel(*refs, z_flips, block, tile, out_tile):
    pieces, refs = refs[:2], refs[2:]
    messages, refs = refs[:PLANE], refs[PLANE:]
    (own_gate, other_gate, own_up, other_up, own_down, other_down), refs = refs[:6], refs[6:]
    outs, (tokens, weight_cols, weights, hidden) = refs[:2], refs[2:]
    half, width = own_down.shape
    positions = weight_cols.shape[1]
    _, depth, core = place()
    for k in range(PLANE):
        weight_cols[k] = column(messages[k][2:3, :positions])
    planes = ((0, plane_flip(core, 0)), (plane_flip(core, 1), PLANE - 1))
    at = 0
    for piece, halves in zip(pieces, planes):
        tokens[at : at + piece.shape[0]] = piece[...]
        for k in halves:
            for z_flip in z_flips:
                source = pl.multiple_of((CORES * (depth ^ z_flip) + core) * block, block)
                weights[at : at + block] = weight_cols[k, pl.ds(source, block)]
                at += block

    for base, gate_w, up_w in ((0, own_gate, own_up), (half, other_gate, other_up)):

        def hide(index, _):
            spot = pl.multiple_of(index * tile, LANES)
            gate = jnp.dot(tokens[...], gate_w[:, pl.ds(spot, tile)], preferred_element_type=F32)
            up = jnp.dot(tokens[...], up_w[:, pl.ds(spot, tile)], preferred_element_type=F32)
            spot = pl.multiple_of(base + spot, LANES)
            hidden[:, pl.ds(spot, tile)] = (jax.nn.silu(gate) * up).astype(BF16)
            return _

        lax.fori_loop(0, half // tile, hide, 0)

    def lower(index, _):
        cols = pl.ds(pl.multiple_of(index * out_tile, LANES), out_tile)
        product = jnp.dot(hidden[:, :half], own_down[:, cols], preferred_element_type=F32)
        product = product + jnp.dot(hidden[:, half:], other_down[:, cols], preferred_element_type=F32)
        scale = jnp.concatenate([weights[...]] * (out_tile // LANES), axis=1)
        scaled = (product * scale).astype(BF16)
        at = 0
        for out in outs:
            out[:, cols] = scaled[at : at + out.shape[0]]
            at += out.shape[0]
        return _

    lax.fori_loop(0, width // out_tile, lower, 0)


def run_experts(pieces, z_flips, messages, weights, block):
    half, width = weights[-1].shape
    rows = sum(piece.shape[0] for piece in pieces)
    positions = block * lax.axis_size("tp")
    return vmem_call(
        functools.partial(
            expert_kernel, z_flips=z_flips, block=block, tile=half, out_tile=width // 2
        ),
        [(piece.shape, BF16) for piece in pieces],
        [*pieces, *messages, *weights],
        scratch=[
            ((rows, width), BF16),
            ((PLANE, positions, LANES), F32),
            ((rows, LANES), F32),
            ((rows, 2 * half), BF16),
        ],
        limit_mib=10,
    )


def float_sum(parts):
    return sum(part.astype(F32) for part in parts)


def spread(rows):
    near = flip_plane(rows, 0)
    pair = jnp.concatenate([rows, near])
    return [pair, flip_plane(pair, 1)]


def gather_sum(outs):
    half = outs[0].shape[0] // 2
    far = flip_plane(outs[1], 1)
    near = float_sum([outs[0][half:], far[half:]]).astype(BF16)
    near = flip_plane(near, 0)
    return float_sum([outs[0][:half], far[:half], near]).astype(BF16)


def local_dense(
    lru_input, gate_input, documents, conv_taps, rate_weight, inlet_weight, decay_param, lru_gain,
    out_weight, residual, ffn_gain, routes, route_weights, w_gate, w_up, w_down,
):
    positions, channels = lru_input.shape
    width = residual.shape[1]
    tp_count = lax.axis_size("tp")
    depths = tp_count // CORES
    block = positions // tp_count
    span = max(positions, channels)

    other_out = flip(out_weight, "tp", 1)

    state, run, mix, *rest = vmem_call(
        lru_kernel,
        [((positions, channels), F32)] * 3
        + [((MESSAGE_ROWS, span), F32)] * PLANE
        + [
            (conv_taps.shape, BF16), (rate_weight.shape, BF16), (inlet_weight.shape, BF16),
            ((1, channels), F32), (out_weight.shape, BF16), ((block, width), BF16),
            (w_down.shape[1:], BF16),
        ],
        [],
        scratch=[
            ((positions, channels), BF16),
            ((positions, channels), BF16),
            ((1, positions), jnp.int32),
            ((1, channels), F32),
            (routes.T.shape, jnp.int32),
            (routes.T.shape, F32),
            ((SUBLANES + positions, channels), F32),
            ((SUBLANES + positions, LANES), F32),
            pltpu.SemaphoreType.DMA((13,)),
        ],
        far_args=[
            lru_input, documents[None, :], conv_taps, rate_weight, inlet_weight,
            decay_param[None, :], gate_input, lru_gain[None, :], routes.T, route_weights.T,
            out_weight, residual, w_down[0],
        ],
    )
    messages, params = rest[:PLANE], rest[PLANE:]
    taps, rate_w, inlet_w, decay_in, own_out, own_residual, own_down = params
    messages = [messages[0]] + [flip(messages[k], "sp", k) for k in range(1, PLANE)]
    early = flip(w_gate[0], "tp", 1)
    messages, other_out, early = lax.optimization_barrier((messages, other_out, early))

    half_rows = positions // CORES
    packed = (half_rows, channels + LANES)
    keep, send = vmem_call(
        functools.partial(mix_kernel, block=block),
        [(packed, BF16)] * 2,
        [state, run, mix, taps, rate_w, inlet_w, decay_in, *messages],
        scratch=[
            ((PLANE, MESSAGE_ROWS, span), F32),
            ((2 * PLANE * SUBLANES, channels), F32),
            ((2 * PLANE * SUBLANES, LANES), F32),
            ((2, PLANE * SUBLANES, channels), F32),
            ((PLANE, SUBLANES, channels), F32),
            ((positions, channels), F32),
            ((positions, channels + LANES), BF16),
        ],
    )
    other, *own = lax.optimization_barrier((flip(send, "tp", 1), w_up[0], w_down[0]))
    swapped = [early] + [flip(value, "tp", 1) for value in own]
    parts = vmem_call(
        functools.partial(project_kernel, block=block),
        [((block, width + LANES), BF16)] * depths,
        [keep, other, own_out, other_out],
        scratch=[(packed, BF16)] * 2,
    )
    parts = dict(enumerate(parts))
    for k in range(depths - 1, 1, -1):
        relay = k & -k
        if relay != k:
            passed = flip_z(parts.pop(k), relay)
            [parts[k ^ relay]] = vmem_call(
                add_kernel, [((block, width + LANES), BF16)], [parts[k ^ relay], passed]
            )
    parts = [parts[k] if k == 0 else flip_z(parts[k], k) for k in parts]
    after, normed = vmem_call(
        functools.partial(norm_kernel, channels_total=channels * tp_count),
        [((block, width), BF16)] * 2,
        [own_residual, ffn_gain[None, :], *parts],
    )

    weights = (w_gate[0], swapped[0], w_up[0], swapped[1], own_down, swapped[2])
    rows_at = [normed] + [flip_z(normed, k) for k in range(1, depths)]
    total = after.astype(F32)
    for k in range(depths):
        pieces = spread(rows_at[k])
        outs = run_experts(pieces, (k,), messages, weights, block)
        summed = gather_sum(outs)
        total = total + (flip_z(summed, k) if k else summed).astype(F32)
    return total.astype(BF16)


def shifted(block, axis, distance):
    devices = range(lax.axis_size(axis))
    route = [(i - distance, i) for i in devices if i - distance in devices]
    return lax.ppermute(block, axis, route)


def carried_in(value, axis, join, neutral):
    count, mine = (lax.axis_size(axis), lax.axis_index(axis))
    pieces = jax.tree.map(lambda part: lax.all_gather(part, axis), value)
    so_far = jax.tree.map(
        lambda part, zero: jnp.full_like(part, 0) + jnp.asarray(zero, part.dtype), value, neutral
    )

    def hop(position, so_far):
        longer = join(so_far, jax.tree.map(lambda part: part[position], pieces))
        return jax.tree.map(lambda new, old: jnp.where(position < mine, new, old), longer, so_far)

    return lax.fori_loop(0, count - 1, hop, so_far)


def join_runs(earlier_run, later_run):
    return (earlier_run[0] * later_run[0], later_run[0] * earlier_run[1] + later_run[1])


def slot_targets(route_block, expert_count, capacity):
    flat_routes = route_block.reshape(-1)
    onehot = (flat_routes[:, None] == jnp.arange(expert_count, dtype=jnp.int32)[None, :]).astype(
        jnp.int32
    )
    earlier_hits = jnp.cumsum(onehot, axis=0) - onehot
    slot_index = jnp.sum(earlier_hits * onehot, axis=1)
    return (flat_routes * capacity + slot_index).reshape(route_block.shape)


def pick_matrix(targets, slot_total):
    slot_hits = targets[None, :, :] == jnp.arange(slot_total, dtype=jnp.int32)[:, None, None]
    return jnp.sum(slot_hits.astype(jnp.int32), axis=2).astype(jnp.bfloat16)


def rms_rows(row_block, gain_vector):
    floated = row_block.astype(jnp.float32)
    inverse_rms = lax.rsqrt(jnp.mean(floated * floated, axis=1, keepdims=True) + EPSILON)
    return (floated * inverse_rms * gain_vector[None, :]).astype(jnp.bfloat16)


def expert_apply(row_piece, gate_weight, up_weight, down_weight):
    gate_part = jnp.dot(row_piece, gate_weight, preferred_element_type=jnp.float32)
    up_part = jnp.dot(row_piece, up_weight, preferred_element_type=jnp.float32)
    hidden_units = (jax.nn.silu(gate_part) * up_part).astype(jnp.bfloat16)
    return jnp.dot(hidden_units, down_weight, preferred_element_type=jnp.float32)


def local_slotted(
    lru_input,
    gate_input,
    documents,
    conv_taps,
    rate_weight,
    inlet_weight,
    decay_param,
    lru_gain,
    out_weight,
    residual,
    ffn_gain,
    routes,
    route_weights,
    w_gate,
    w_up,
    w_down,
):
    positions = lru_input.shape[0]
    channels = lru_input.shape[1]
    model_width = residual.shape[1]
    reach_back = conv_taps.shape[0] - 1
    tail_rows, tail_docs = shifted(
        (lru_input[positions - reach_back :], documents[positions - reach_back :] + 1), "sp", 1
    )
    prior_docs = jnp.concatenate([tail_docs - 1, documents])
    padded_input = jnp.concatenate([tail_rows, lru_input], axis=0)
    conv_sum = jnp.zeros((positions, channels), jnp.float32)
    for tap_index in range(reach_back + 1):
        same_doc = (prior_docs[tap_index : tap_index + positions] == documents).astype(jnp.float32)[
            :, None
        ]
        conv_sum = (
            conv_sum
            + padded_input[tap_index : tap_index + positions].astype(jnp.float32)
            * conv_taps[tap_index].astype(jnp.float32)[None, :]
            * same_doc
        )
    convolved = conv_sum.astype(jnp.bfloat16)
    grouped = convolved.reshape(positions, rate_weight.shape[0], rate_weight.shape[1])
    rate_gate = jax.nn.sigmoid(
        jnp.einsum(
            "tnc,ncd->tnd", grouped, rate_weight, preferred_element_type=jnp.float32
        ).reshape(positions, channels)
    )
    inlet_gate = jax.nn.sigmoid(
        jnp.einsum(
            "tnc,ncd->tnd", grouped, inlet_weight, preferred_element_type=jnp.float32
        ).reshape(positions, channels)
    )
    log_decay = -RATE_SCALE * rate_gate * jax.nn.softplus(-decay_param)[None, :]
    starts = (prior_docs[reach_back - 1 : reach_back - 1 + positions] != documents)[:, None]
    decay_step = jnp.where(starts, 0.0, jnp.exp(log_decay))
    norm_factor = jnp.where(starts, 1.0, jnp.sqrt(-jnp.expm1(2.0 * log_decay)))
    drive_term = norm_factor * inlet_gate * convolved.astype(jnp.float32)
    decay_run, local_state = lax.associative_scan(join_runs, (decay_step, drive_term), axis=0)
    carried = carried_in(
        (decay_run[positions - 1], local_state[positions - 1]),
        "sp",
        join_runs,
        (jnp.ones((channels,), jnp.float32), jnp.zeros((channels,), jnp.float32)),
    )
    hidden_state = local_state + decay_run * carried[1][None, :]
    square_sums = lax.psum(jnp.sum(hidden_state * hidden_state, axis=1), "tp")
    inverse_rms = lax.rsqrt(square_sums[:, None] / (channels * lax.axis_size("tp")) + EPSILON)
    mixer_rows = (
        hidden_state * inverse_rms * lru_gain[None, :] * jax.nn.gelu(gate_input.astype(jnp.float32))
    ).astype(jnp.bfloat16)
    tp_count = lax.axis_size("tp")
    tp_here = lax.axis_index("tp")
    expert_count = lax.axis_size("sp")
    route_rows = positions // tp_count
    top_count = routes.shape[1]
    capacity = 2 * top_count * route_rows // expert_count
    slot_total = expert_count * capacity
    projected = lax.psum_scatter(
        jnp.dot(mixer_rows, out_weight, preferred_element_type=jnp.float32).astype(jnp.bfloat16),
        "tp",
        scatter_dimension=0,
        tiled=True,
    ).astype(jnp.float32)
    own_rows = (
        lax.dynamic_slice_in_dim(residual, tp_here * route_rows, route_rows, 0).astype(jnp.float32)
        + projected
    ).astype(jnp.bfloat16)
    own_routes = lax.dynamic_slice_in_dim(routes, tp_here * route_rows, route_rows, 0)
    targets = slot_targets(own_routes, expert_count, capacity)
    outgoing = jnp.dot(
        pick_matrix(targets, slot_total),
        rms_rows(own_rows, ffn_gain),
        preferred_element_type=jnp.float32,
    ).astype(jnp.bfloat16)
    arrived = lax.all_to_all(
        outgoing.reshape(expert_count, capacity, model_width),
        "sp",
        split_axis=0,
        concat_axis=0,
        tiled=True,
    )
    partial_out = expert_apply(
        lax.all_gather(arrived.reshape(slot_total, model_width), "tp", axis=0, tiled=True),
        w_gate[0],
        w_up[0],
        w_down[0],
    )
    expert_out = lax.psum_scatter(
        partial_out.astype(jnp.bfloat16), "tp", scatter_dimension=0, tiled=True
    )
    returned = lax.all_to_all(
        expert_out.reshape(expert_count, capacity, model_width),
        "sp",
        split_axis=0,
        concat_axis=0,
        tiled=True,
    )
    picked = returned.reshape(slot_total, model_width)[targets.reshape(-1)].astype(jnp.float32)
    picked = picked.reshape(route_rows, top_count, model_width)
    own_weights = lax.dynamic_slice_in_dim(route_weights, tp_here * route_rows, route_rows, 0)
    routed = jnp.sum(picked * own_weights[:, :, None], axis=1)
    return (own_rows.astype(jnp.float32) + routed).astype(jnp.bfloat16)


def local(*arrays):
    positions, top_count = arrays[11].shape
    shards = lax.axis_size("sp")
    route_rows = positions // lax.axis_size("tp")
    dense = shards == PLANE and 2 * top_count * route_rows // shards >= route_rows
    if not dense:
        return local_slotted(*arrays)
    return local_dense(*arrays)


def solution(mesh):
    return jax.shard_map(
        local,
        mesh=mesh,
        in_specs=(
            P("sp", "tp"),
            P("sp", "tp"),
            P("sp"),
            P(None, "tp"),
            P("tp", None, None),
            P("tp", None, None),
            P("tp"),
            P("tp"),
            P("tp", None),
            P("sp", None),
            P(),
            P("sp", None),
            P("sp", None),
            P("sp", None, "tp"),
            P("sp", None, "tp"),
            P("sp", "tp", None),
        ),
        out_specs=P(("sp", "tp"), None),
        check_vma=False,
    )
```

profile of v0, /device:TPU:0, one launch (start us, length us, event | category | flops | bytes accessed | tf_op | source)
XLA Modules:
  0.0 92.9 jit_solution(4330553282664460523)
XLA Ops:
  0.0 0.5 collective-permute-start.4
  0.5 2.8 %shard_map.154 = (f32[256,256]{1,0:T(8,128)S(1)}, f32[256,256]{1,0:T(8,128)S(1)}, f32[256,256]{1,0:T(8,128)S(1)}, f32[24,256]{1,0:T(8,128)S(1)}, f32[24,256]{1,0...) custom-call(bf16[256,256]{1,0:T(8,128)(2,1)} %refs_0_.1, ...), custom_call_target="tpu_custom_call" | custom-call | tf_op jit(solution)/shard_map/pallas_call | solution.py:25
  3.3 3.0 %collective-permute-start = (f32[24,256]{1,0:T(8,128)S(1)}, f32[24,256]{1,0:T(8,128)S(1)}, u32[]{:S(2)}, u32[]{:S(2)}) collective-permute-start(f32[24,256]{1,0:T(8,128)S(1)} %get-tuple-element.53), channel_id=1, source_target_pairs={{0,8},{8,0},{16,24},{24,16},{1,9},{9,1},{17,25},{25,17},{2,10},{10... | collective-permute-start | bytes 73736 | tf_op jit(solution)/shard_map/ppermute | solution.py:46
  6.3 1.5 %collective-permute-start.1 = (f32[24,256]{1,0:T(8,128)S(1)}, f32[24,256]{1,0:T(8,128)S(1)}, u32[]{:S(2)}, u32[]{:S(2)}) collective-permute-start(f32[24,256]{1,0:T(8,128)S(1)} %get-tuple-element.54), channel_id=1, source_target_pairs={{0,16},{8,24},{16,0},{24,8},{1,17},{9,25},{17,1},{25,9},{2,18},{10... | collective-permute-start | bytes 73736 | tf_op jit(solution)/shard_map/ppermute | solution.py:46
  8.1 2.0 %collective-permute-done.1.rest_2_.refs_4_ = f32[24,256]{1,0:T(8,128)S(1)} collective-permute-done((f32[24,256]{1,0:T(8,128)S(1)}, f32[24,256]{1,0:T(8,128)S(1)}, u32[]{:S(2)}, u32[]{:S(2)}) %collective-permute-start.1) | collective-permute-done | bytes 24608 | tf_op jit(solution)/shard_map/ppermute | solution.py:46
  10.2 2.4 %collective-permute-done.2.rest_3_.refs_5_ = f32[24,256]{1,0:T(8,128)S(1)} collective-permute-done((f32[24,256]{1,0:T(8,128)S(1)}, f32[24,256]{1,0:T(8,128)S(1)}, u32[]{:S(2)}, u32[]{:S(2)}) %collective-permute-start.2) | collective-permute-done | bytes 24608 | tf_op jit(solution)/shard_map/ppermute | solution.py:46
  13.1 1.3 %collective-permute-done.5.other = bf16[128,384]{1,0:T(8,128)(2,1)S(1)} collective-permute-done((bf16[128,384]{1,0:T(8,128)(2,1)S(1)}, bf16[128,384]{1,0:T(8,128)(2,1)S(1)}, u32[]{:S(2)}, u32[]{:S(2)}) %collective-permute-start.5) | collective-permute-done | bytes 98336 | tf_op jit(solution)/shard_map/ppermute | solution.py:46
  14.9 0.5 shard_map.156
  15.4 1.6 %collective-permute-start.7 = (bf16[32,2176]{1,0:T(8,128)(2,1)S(1)}, bf16[32,2176]{1,0:T(8,128)(2,1)S(1)}, u32[]{:S(2)}, u32[]{:S(2)}) collective-permute-start(bf16[32,2176]{1,0:T(8,128)(2,1)S(1)} %get-tuple-element.68), channel_id=1, source_target_pairs={{0,2},{1,3},{2,0},{3,1},{4,6},{5,7},{6,4},{7,5},{8,10},{9,11},{10,... | collective-permute-start | bytes 417800 | tf_op jit(solution)/shard_map/ppermute | solution.py:46
  17.0 0.5 collective-permute-start.6
  17.4 4.5 %collective-permute-done.7.two = bf16[32,2176]{1,0:T(8,128)(2,1)S(1)} collective-permute-done((bf16[32,2176]{1,0:T(8,128)(2,1)S(1)}, bf16[32,2176]{1,0:T(8,128)(2,1)S(1)}, u32[]{:S(2)}, u32[]{:S(2)}) %collective-permute-start.7) | collective-permute-done | bytes 139296 | tf_op jit(solution)/shard_map/ppermute | solution.py:46
  22.1 2.6 %collective-permute-start.8 = (bf16[32,2176]{1,0:T(8,128)(2,1)S(1)}, bf16[32,2176]{1,0:T(8,128)(2,1)S(1)}, u32[]{:S(2)}, u32[]{:S(2)}) collective-permute-start(bf16[32,2176]{1,0:T(8,128)(2,1)S(1)} %shard_map.157), channel_id=1, source_target_pairs={{0,4},{1,5},{2,6},{3,7},{4,0},{5,1},{6,2},{7,3},{8,12},{9,13},{10,... | collective-permute-start | bytes 417800 | tf_op jit(solution)/shard_map/ppermute | solution.py:46
  24.8 5.7 %collective-permute-done.8.rest_2_ = bf16[32,2176]{1,0:T(8,128)(2,1)S(1)} collective-permute-done((bf16[32,2176]{1,0:T(8,128)(2,1)S(1)}, bf16[32,2176]{1,0:T(8,128)(2,1)S(1)}, u32[]{:S(2)}, u32[]{:S(2)}) %collective-permute-start.8) | collective-permute-done | bytes 139296 | tf_op jit(solution)/shard_map/ppermute | solution.py:46
  30.8 3.5 %collective-permute-start.27 = (bf16[32,2048]{1,0:T(8,128)(2,1)S(1)}, bf16[32,2048]{1,0:T(8,128)(2,1)S(1)}, u32[]{:S(2)}, u32[]{:S(2)}) collective-permute-start(bf16[32,2048]{1,0:T(8,128)(2,1)S(1)} %get-tuple-element.70), channel_id=1, source_target_pairs={{0,6},{1,7},{2,4},{3,5},{4,2},{5,3},{6,0},{7,1},{8,14},{9,15},{10,... | collective-permute-start | bytes 393224 | tf_op jit(solution)/shard_map/ppermute | solution.py:46
  34.3 0.9 collective-permute-start.15
  35.2 3.5 %collective-permute-done.27 = bf16[32,2048]{1,0:T(8,128)(2,1)S(1)} collective-permute-done((bf16[32,2048]{1,0:T(8,128)(2,1)S(1)}, bf16[32,2048]{1,0:T(8,128)(2,1)S(1)}, u32[]{:S(2)}, u32[]{:S(2)}) %collective-permute-start.27) | collective-permute-done | bytes 131104 | tf_op jit(solution)/shard_map/ppermute | solution.py:46
  38.8 0.6 collective-permute-start.9
  39.3 4.3 %collective-permute-done.21 = bf16[32,2048]{1,0:T(8,128)(2,1)S(1)} collective-permute-done((bf16[32,2048]{1,0:T(8,128)(2,1)S(1)}, bf16[32,2048]{1,0:T(8,128)(2,1)S(1)}, u32[]{:S(2)}, u32[]{:S(2)}) %collective-permute-start.21) | collective-permute-done | bytes 131104 | tf_op jit(solution)/shard_map/ppermute | solution.py:46
  43.6 0.6 collective-permute-start.28
  44.2 1.5 %collective-permute-start.22 = (bf16[32,2048]{1,0:T(8,128)(2,1)S(1)}, bf16[32,2048]{1,0:T(8,128)(2,1)S(1)}, u32[]{:S(2)}, u32[]{:S(2)}) collective-permute-start(bf16[32,2048]{1,0:T(8,128)(2,1)S(1)} %collective-permute-done.21), channel_id=1, source_target_pairs={{0,8},{1,17},{2,10},{3,19},{4,12},{5,21},{6,14},{7,23},{8,0},{9,25... | collective-permute-start | bytes 393224 | tf_op jit(solution)/shard_map/ppermute | solution.py:56
  45.8 0.6 collective-permute-start.16
  46.4 2.2 %collective-permute-done.28 = bf16[32,2048]{1,0:T(8,128)(2,1)S(1)} collective-permute-done((bf16[32,2048]{1,0:T(8,128)(2,1)S(1)}, bf16[32,2048]{1,0:T(8,128)(2,1)S(1)}, u32[]{:S(2)}, u32[]{:S(2)}) %collective-permute-start.28) | collective-permute-done | bytes 131104 | tf_op jit(solution)/shard_map/ppermute | solution.py:56
  48.6 0.6 collective-permute-start.29
  49.2 1.9 %collective-permute-done.22 = bf16[32,2048]{1,0:T(8,128)(2,1)S(1)} collective-permute-done((bf16[32,2048]{1,0:T(8,128)(2,1)S(1)}, bf16[32,2048]{1,0:T(8,128)(2,1)S(1)}, u32[]{:S(2)}, u32[]{:S(2)}) %collective-permute-start.22) | collective-permute-done | bytes 131104 | tf_op jit(solution)/shard_map/ppermute | solution.py:56
  51.1 0.6 collective-permute-start.23
  51.7 2.2 %collective-permute-done.16 = bf16[32,2048]{1,0:T(8,128)(2,1)S(1)} collective-permute-done((bf16[32,2048]{1,0:T(8,128)(2,1)S(1)}, bf16[32,2048]{1,0:T(8,128)(2,1)S(1)}, u32[]{:S(2)}, u32[]{:S(2)}) %collective-permute-start.16) | collective-permute-done | bytes 131104 | tf_op jit(solution)/shard_map/ppermute | solution.py:56
  53.9 0.6 collective-permute-start.17
  54.5 0.6 collective-permute-done.29.refs_1_
  55.0 0.9 %collective-permute-start.10 = (bf16[64,2048]{1,0:T(8,128)(2,1)S(1)}, bf16[64,2048]{1,0:T(8,128)(2,1)S(1)}, u32[]{:S(2)}, u32[]{:S(2)}) collective-permute-start(bf16[64,2048]{1,0:T(8,128)(2,1)S(1)} %constant_dynamic-update-slice_fusion.refs_0_), channel_id=1, source_target_pairs={{0,16},{1,9},{2,18},{3,11},{4,20},{5,13},{6,22},{7,15},{8,24},{9,1... | collective-permute-start | bytes 786440 | tf_op jit(solution)/shard_map/ppermute | solution.py:56
  56.0 3.2 %shard_map.162 = (bf16[64,2048]{1,0:T(8,128)(2,1)S(1)}, bf16[64,2048]{1,0:T(8,128)(2,1)S(1)}) custom-call(bf16[64,2048]{1,0:T(8,128)(2,1)S(1)} %constant_dynamic-update-slice_fusion.6.refs_0_, bf16[64,2048]{1,0:T(8,128)(2,1)S(1)} %collective-permute-done.29.refs_1_, f32[24,256]{1,0:T(8,128)S(1)} %get-tuple-element.56.rest_0_.refs_2_, ...), custom_call_target="tpu_custom_call" | custom-call | tf_op jit(solution)/shard_map/pallas_call | solution.py:25
  59.2 1.1 %collective-permute-start.30 = (bf16[64,2048]{1,0:T(8,128)(2,1)S(1)}, bf16[64,2048]{1,0:T(8,128)(2,1)S(1)}, u32[]{:S(2)}, u32[]{:S(2)}) collective-permute-start(bf16[64,2048]{1,0:T(8,128)(2,1)S(1)} %get-tuple-element.82), channel_id=1, source_target_pairs={{0,16},{1,9},{2,18},{3,11},{4,20},{5,13},{6,22},{7,15},{8,24},{9,1... | collective-permute-start | bytes 786440 | tf_op jit(solution)/shard_map/ppermute | solution.py:56
  60.3 3.0 %shard_map.161 = (bf16[64,2048]{1,0:T(8,128)(2,1)S(1)}, bf16[64,2048]{1,0:T(8,128)(2,1)S(1)}) custom-call(bf16[64,2048]{1,0:T(8,128)(2,1)S(1)} %constant_dynamic-update-slice_fusion.4.refs_0_, bf16[64,2048]{1,0:T(8,128)(2,1)S(1)} %collective-permute-done.23.refs_1_, f32[24,256]{1,0:T(8,128)S(1)} %get-tuple-element.56.rest_0_.refs_2_, ...), custom_call_target="tpu_custom_call" | custom-call | tf_op jit(solution)/shard_map/pallas_call | solution.py:25
  63.3 1.0 %collective-permute-start.24 = (bf16[64,2048]{1,0:T(8,128)(2,1)S(1)}, bf16[64,2048]{1,0:T(8,128)(2,1)S(1)}, u32[]{:S(2)}, u32[]{:S(2)}) collective-permute-start(bf16[64,2048]{1,0:T(8,128)(2,1)S(1)} %get-tuple-element.80), channel_id=1, source_target_pairs={{0,16},{1,9},{2,18},{3,11},{4,20},{5,13},{6,22},{7,15},{8,24},{9,1... | collective-permute-start | bytes 786440 | tf_op jit(solution)/shard_map/ppermute | solution.py:56
  64.4 3.0 %shard_map.160 = (bf16[64,2048]{1,0:T(8,128)(2,1)S(1)}, bf16[64,2048]{1,0:T(8,128)(2,1)S(1)}) custom-call(bf16[64,2048]{1,0:T(8,128)(2,1)S(1)} %constant_dynamic-update-slice_fusion.2.refs_0_, bf16[64,2048]{1,0:T(8,128)(2,1)S(1)} %collective-permute-done.17.refs_1_, f32[24,256]{1,0:T(8,128)S(1)} %get-tuple-element.56.rest_0_.refs_2_, ...), custom_call_target="tpu_custom_call" | custom-call | tf_op jit(solution)/shard_map/pallas_call | solution.py:25
  67.4 1.1 %collective-permute-start.18 = (bf16[64,2048]{1,0:T(8,128)(2,1)S(1)}, bf16[64,2048]{1,0:T(8,128)(2,1)S(1)}, u32[]{:S(2)}, u32[]{:S(2)}) collective-permute-start(bf16[64,2048]{1,0:T(8,128)(2,1)S(1)} %get-tuple-element.78), channel_id=1, source_target_pairs={{0,16},{1,9},{2,18},{3,11},{4,20},{5,13},{6,22},{7,15},{8,24},{9,1... | collective-permute-start | bytes 786440 | tf_op jit(solution)/shard_map/ppermute | solution.py:56
  68.5 3.0 %shard_map.159 = (bf16[64,2048]{1,0:T(8,128)(2,1)S(1)}, bf16[64,2048]{1,0:T(8,128)(2,1)S(1)}) custom-call(bf16[64,2048]{1,0:T(8,128)(2,1)S(1)} %constant_dynamic-update-slice_fusion.refs_0_, bf16[64,2048]{1,0:T(8,128)(2,1)S(1)} %collective-permute-done.10.refs_1_, f32[24,256]{1,0:T(8,128)S(1)} %get-tuple-element.56.rest_0_.refs_2_, ...), custom_call_target="tpu_custom_call" | custom-call | tf_op jit(solution)/shard_map/pallas_call | solution.py:25
  71.5 1.0 %collective-permute-start.13 = (bf16[64,2048]{1,0:T(8,128)(2,1)S(1)}, bf16[64,2048]{1,0:T(8,128)(2,1)S(1)}, u32[]{:S(2)}, u32[]{:S(2)}) collective-permute-start(bf16[64,2048]{1,0:T(8,128)(2,1)S(1)} %get-tuple-element.76), channel_id=1, source_target_pairs={{0,16},{1,9},{2,18},{3,11},{4,20},{5,13},{6,22},{7,15},{8,24},{9,1... | collective-permute-start | bytes 786440 | tf_op jit(solution)/shard_map/ppermute | solution.py:56
  72.6 0.9 collective-permute-start.31
  73.5 1.3 %collective-permute-start.25 = (bf16[32,2048]{1,0:T(8,128)(2,1)S(1)}, bf16[32,2048]{1,0:T(8,128)(2,1)S(1)}, u32[]{:S(2)}, u32[]{:S(2)}) collective-permute-start(bf16[32,2048]{1,0:T(8,128)(2,1)S(1)} %add_convert_fusion.4), channel_id=1, source_target_pairs={{0,8},{1,17},{2,10},{3,19},{4,12},{5,21},{6,14},{7,23},{8,0},{9,25... | collective-permute-start | bytes 393224 | tf_op jit(solution)/shard_map/ppermute | solution.py:56
  74.8 0.9 collective-permute-start.19
  75.7 5.0 %collective-permute-done.13 = bf16[64,2048]{1,0:T(8,128)(2,1)S(1)} collective-permute-done((bf16[64,2048]{1,0:T(8,128)(2,1)S(1)}, bf16[64,2048]{1,0:T(8,128)(2,1)S(1)}, u32[]{:S(2)}, u32[]{:S(2)}) %collective-permute-start.13) | collective-permute-done | bytes 262176 | tf_op jit(solution)/shard_map/ppermute | solution.py:56
  80.8 0.6 collective-permute-start.14
  81.5 1.9 %collective-permute-start.32 = (bf16[32,2048]{1,0:T(8,128)(2,1)S(1)}, bf16[32,2048]{1,0:T(8,128)(2,1)S(1)}, u32[]{:S(2)}, u32[]{:S(2)}) collective-permute-start(bf16[32,2048]{1,0:T(8,128)(2,1)S(1)} %add_convert_fusion.1), channel_id=1, source_target_pairs={{0,6},{1,7},{2,4},{3,5},{4,2},{5,3},{6,0},{7,1},{8,14},{9,15},{10,... | collective-permute-start | bytes 393224 | tf_op jit(solution)/shard_map/ppermute | solution.py:46
  83.4 1.6 %collective-permute-start.26 = (bf16[32,2048]{1,0:T(8,128)(2,1)S(1)}, bf16[32,2048]{1,0:T(8,128)(2,1)S(1)}, u32[]{:S(2)}, u32[]{:S(2)}) collective-permute-start(bf16[32,2048]{1,0:T(8,128)(2,1)S(1)} %add_convert_fusion.3), channel_id=1, source_target_pairs={{0,4},{1,5},{2,6},{3,7},{4,0},{5,1},{6,2},{7,3},{8,12},{9,13},{10,... | collective-permute-start | bytes 393224 | tf_op jit(solution)/shard_map/ppermute | solution.py:46
  85.1 1.1 %collective-permute-start.20 = (bf16[32,2048]{1,0:T(8,128)(2,1)S(1)}, bf16[32,2048]{1,0:T(8,128)(2,1)S(1)}, u32[]{:S(2)}, u32[]{:S(2)}) collective-permute-start(bf16[32,2048]{1,0:T(8,128)(2,1)S(1)} %add_convert_fusion.5), channel_id=1, source_target_pairs={{0,2},{1,3},{2,0},{3,1},{4,6},{5,7},{6,4},{7,5},{8,10},{9,11},{10,... | collective-permute-start | bytes 393224 | tf_op jit(solution)/shard_map/ppermute | solution.py:46
  86.2 2.2 %collective-permute-done.32 = bf16[32,2048]{1,0:T(8,128)(2,1)S(1)} collective-permute-done((bf16[32,2048]{1,0:T(8,128)(2,1)S(1)}, bf16[32,2048]{1,0:T(8,128)(2,1)S(1)}, u32[]{:S(2)}, u32[]{:S(2)}) %collective-permute-start.32) | collective-permute-done | bytes 131104 | tf_op jit(solution)/shard_map/ppermute | solution.py:46
  88.4 3.7 %collective-permute-done.26 = bf16[32,2048]{1,0:T(8,128)(2,1)S(1)} collective-permute-done((bf16[32,2048]{1,0:T(8,128)(2,1)S(1)}, bf16[32,2048]{1,0:T(8,128)(2,1)S(1)}, u32[]{:S(2)}, u32[]{:S(2)}) %collective-permute-start.26) | collective-permute-done | bytes 131104 | tf_op jit(solution)/shard_map/ppermute | solution.py:46
  92.1 0.8 add_convert_fusion
  (51 shorter events, 2.2 us)
Async XLA Ops:
  0.0 12.6 %collective-permute-start.4 = (bf16[2048,768]{1,0:T(8,128)(2,1)}, bf16[2048,768]{1,0:T(8,128)(2,1)S(1)}, u32[]{:S(2)}, u32[]{:S(2)}) collective-permute-start(bf16[2048,768]{1,0:T(8,128)(2,1)} %bitcast.9), channel_id=1, source_target_pairs={{0,1},{1,0},{2,3},{3,2},{4,5},{5,4},{6,7},{7,6},{8,9},{9,8},{10,11... | collective-permute-start | bytes 9437192 | tf_op jit(solution)/shard_map/ppermute | solution.py:46
  0.5 12.1 %collective-permute-start.3 = (bf16[256,2048]{1,0:T(8,128)(2,1)}, bf16[256,2048]{1,0:T(8,128)(2,1)S(1)}, u32[]{:S(2)}, u32[]{:S(2)}) collective-permute-start(bf16[256,2048]{1,0:T(8,128)(2,1)} %refs_10_.1), channel_id=1, source_target_pairs={{0,1},{1,0},{2,3},{3,2},{4,5},{5,4},{6,7},{7,6},{8,9},{9,8},{10,11... | collective-permute-start | bytes 3145736 | tf_op jit(solution)/shard_map/ppermute | solution.py:46
  0.5 13.9 %copy-start.1 = (bf16[1,2048,768]{2,1,0:T(8,128)(2,1)S(1)}, bf16[1,2048,768]{2,1,0:T(8,128)(2,1)}, u32[]{:S(2)}) copy-start(bf16[1,2048,768]{2,1,0:T(8,128)(2,1)} %param.30) | copy-start | bytes 9437188
  0.5 14.0 %copy-start.3 = (bf16[1,768,2048]{2,1,0:T(8,128)(2,1)S(1)}, bf16[1,768,2048]{2,1,0:T(8,128)(2,1)}, u32[]{:S(2)}) copy-start(bf16[1,768,2048]{2,1,0:T(8,128)(2,1)} %param.31) | copy-start | bytes 9437188
  3.3 27.2 %copy-start.2 = (f32[2048]{0:T(1024)S(1)}, f32[2048]{0:T(1024)}, u32[]{:S(2)}) copy-start(f32[2048]{0:T(1024)} %param.26) | copy-start | bytes 24580
  3.3 4.8 %collective-permute-start = (f32[24,256]{1,0:T(8,128)S(1)}, f32[24,256]{1,0:T(8,128)S(1)}, u32[]{:S(2)}, u32[]{:S(2)}) collective-permute-start(f32[24,256]{1,0:T(8,128)S(1)} %get-tuple-element.53), channel_id=1, source_target_pairs={{0,8},{8,0},{16,24},{24,16},{1,9},{9,1},{17,25},{25,17},{2,10},{10... | collective-permute-start | bytes 73736 | tf_op jit(solution)/shard_map/ppermute | solution.py:46
  6.3 3.8 %collective-permute-start.1 = (f32[24,256]{1,0:T(8,128)S(1)}, f32[24,256]{1,0:T(8,128)S(1)}, u32[]{:S(2)}, u32[]{:S(2)}) collective-permute-start(f32[24,256]{1,0:T(8,128)S(1)} %get-tuple-element.54), channel_id=1, source_target_pairs={{0,16},{8,24},{16,0},{24,8},{1,17},{9,25},{17,1},{25,9},{2,18},{10... | collective-permute-start | bytes 73736 | tf_op jit(solution)/shard_map/ppermute | solution.py:46
  7.8 4.7 %collective-permute-start.2 = (f32[24,256]{1,0:T(8,128)S(1)}, f32[24,256]{1,0:T(8,128)S(1)}, u32[]{:S(2)}, u32[]{:S(2)}) collective-permute-start(f32[24,256]{1,0:T(8,128)S(1)} %get-tuple-element.55), channel_id=1, source_target_pairs={{0,24},{8,16},{16,8},{24,0},{1,25},{9,17},{17,9},{25,1},{2,26},{10... | collective-permute-start | bytes 73736 | tf_op jit(solution)/shard_map/ppermute | solution.py:46
  12.6 43.4 %copy-start = (bf16[1,2048,768]{2,1,0:T(8,128)(2,1)S(1)}, bf16[1,2048,768]{2,1,0:T(8,128)(2,1)}, u32[]{:S(2)}) copy-start(bf16[1,2048,768]{2,1,0:T(8,128)(2,1)} %param.29) | copy-start | bytes 9437188
  13.0 1.4 %collective-permute-start.5 = (bf16[128,384]{1,0:T(8,128)(2,1)S(1)}, bf16[128,384]{1,0:T(8,128)(2,1)S(1)}, u32[]{:S(2)}, u32[]{:S(2)}) collective-permute-start(bf16[128,384]{1,0:T(8,128)(2,1)S(1)} %get-tuple-element.61), channel_id=1, source_target_pairs={{0,1},{1,0},{2,3},{3,2},{4,5},{5,4},{6,7},{7,6},{8,9},{9,8},{10,11... | collective-permute-start | bytes 294920 | tf_op jit(solution)/shard_map/ppermute | solution.py:46
  14.4 41.6 %collective-permute-start.11 = (bf16[2048,768]{1,0:T(8,128)(2,1)S(1)}, bf16[2048,768]{1,0:T(8,128)(2,1)S(1)}, u32[]{:S(2)}, u32[]{:S(2)}) collective-permute-start(bf16[2048,768]{1,0:T(8,128)(2,1)S(1)} %bitcast.14), channel_id=1, source_target_pairs={{0,1},{1,0},{2,3},{3,2},{4,5},{5,4},{6,7},{7,6},{8,9},{9,8},{10,11... | collective-permute-start | bytes 9437192 | tf_op jit(solution)/shard_map/ppermute | solution.py:46
  14.5 41.5 %collective-permute-start.12 = (bf16[768,2048]{1,0:T(8,128)(2,1)S(1)}, bf16[768,2048]{1,0:T(8,128)(2,1)S(1)}, u32[]{:S(2)}, u32[]{:S(2)}) collective-permute-start(bf16[768,2048]{1,0:T(8,128)(2,1)S(1)} %bitcast.21), channel_id=1, source_target_pairs={{0,1},{1,0},{2,3},{3,2},{4,5},{5,4},{6,7},{7,6},{8,9},{9,8},{10,11... | collective-permute-start | bytes 9437192 | tf_op jit(solution)/shard_map/ppermute | solution.py:46
  15.4 6.6 %collective-permute-start.7 = (bf16[32,2176]{1,0:T(8,128)(2,1)S(1)}, bf16[32,2176]{1,0:T(8,128)(2,1)S(1)}, u32[]{:S(2)}, u32[]{:S(2)}) collective-permute-start(bf16[32,2176]{1,0:T(8,128)(2,1)S(1)} %get-tuple-element.68), channel_id=1, source_target_pairs={{0,2},{1,3},{2,0},{3,1},{4,6},{5,7},{6,4},{7,5},{8,10},{9,11},{10,... | collective-permute-start | bytes 417800 | tf_op jit(solution)/shard_map/ppermute | solution.py:46
  17.0 7.8 %collective-permute-start.6 = (bf16[32,2176]{1,0:T(8,128)(2,1)S(1)}, bf16[32,2176]{1,0:T(8,128)(2,1)S(1)}, u32[]{:S(2)}, u32[]{:S(2)}) collective-permute-start(bf16[32,2176]{1,0:T(8,128)(2,1)S(1)} %get-tuple-element.66), channel_id=1, source_target_pairs={{0,2},{1,3},{2,0},{3,1},{4,6},{5,7},{6,4},{7,5},{8,10},{9,11},{10,... | collective-permute-start | bytes 417800 | tf_op jit(solution)/shard_map/ppermute | solution.py:46
  22.1 8.3 %collective-permute-start.8 = (bf16[32,2176]{1,0:T(8,128)(2,1)S(1)}, bf16[32,2176]{1,0:T(8,128)(2,1)S(1)}, u32[]{:S(2)}, u32[]{:S(2)}) collective-permute-start(bf16[32,2176]{1,0:T(8,128)(2,1)S(1)} %shard_map.157), channel_id=1, source_target_pairs={{0,4},{1,5},{2,6},{3,7},{4,0},{5,1},{6,2},{7,3},{8,12},{9,13},{10,... | collective-permute-start | bytes 417800 | tf_op jit(solution)/shard_map/ppermute | solution.py:46
  30.8 8.0 %collective-permute-start.27 = (bf16[32,2048]{1,0:T(8,128)(2,1)S(1)}, bf16[32,2048]{1,0:T(8,128)(2,1)S(1)}, u32[]{:S(2)}, u32[]{:S(2)}) collective-permute-start(bf16[32,2048]{1,0:T(8,128)(2,1)S(1)} %get-tuple-element.70), channel_id=1, source_target_pairs={{0,6},{1,7},{2,4},{3,5},{4,2},{5,3},{6,0},{7,1},{8,14},{9,15},{10,... | collective-permute-start | bytes 393224 | tf_op jit(solution)/shard_map/ppermute | solution.py:46
  34.3 9.3 %collective-permute-start.21 = (bf16[32,2048]{1,0:T(8,128)(2,1)S(1)}, bf16[32,2048]{1,0:T(8,128)(2,1)S(1)}, u32[]{:S(2)}, u32[]{:S(2)}) collective-permute-start(bf16[32,2048]{1,0:T(8,128)(2,1)S(1)} %get-tuple-element.70), channel_id=1, source_target_pairs={{0,4},{1,5},{2,6},{3,7},{4,0},{5,1},{6,2},{7,3},{8,12},{9,13},{10,... | collective-permute-start | bytes 393224 | tf_op jit(solution)/shard_map/ppermute | solution.py:46
  34.3 9.9 %collective-permute-start.15 = (bf16[32,2048]{1,0:T(8,128)(2,1)S(1)}, bf16[32,2048]{1,0:T(8,128)(2,1)S(1)}, u32[]{:S(2)}, u32[]{:S(2)}) collective-permute-start(bf16[32,2048]{1,0:T(8,128)(2,1)S(1)} %get-tuple-element.70), channel_id=1, source_target_pairs={{0,2},{1,3},{2,0},{3,1},{4,6},{5,7},{6,4},{7,5},{8,10},{9,11},{10,... | collective-permute-start | bytes 393224 | tf_op jit(solution)/shard_map/ppermute | solution.py:46
  38.8 7.0 %collective-permute-start.9 = (bf16[32,2048]{1,0:T(8,128)(2,1)S(1)}, bf16[32,2048]{1,0:T(8,128)(2,1)S(1)}, u32[]{:S(2)}, u32[]{:S(2)}) collective-permute-start(bf16[32,2048]{1,0:T(8,128)(2,1)S(1)} %get-tuple-element.70), channel_id=1, source_target_pairs={{0,8},{1,17},{2,10},{3,19},{4,12},{5,21},{6,14},{7,23},{8,0},{9,25... | collective-permute-start | bytes 393224 | tf_op jit(solution)/shard_map/ppermute | solution.py:56
  43.6 5.0 %collective-permute-start.28 = (bf16[32,2048]{1,0:T(8,128)(2,1)S(1)}, bf16[32,2048]{1,0:T(8,128)(2,1)S(1)}, u32[]{:S(2)}, u32[]{:S(2)}) collective-permute-start(bf16[32,2048]{1,0:T(8,128)(2,1)S(1)} %collective-permute-done.27), channel_id=1, source_target_pairs={{0,8},{1,17},{2,10},{3,19},{4,12},{5,21},{6,14},{7,23},{8,0},{9,25... | collective-permute-start | bytes 393224 | tf_op jit(solution)/shard_map/ppermute | solution.py:56
  44.2 6.8 %collective-permute-start.22 = (bf16[32,2048]{1,0:T(8,128)(2,1)S(1)}, bf16[32,2048]{1,0:T(8,128)(2,1)S(1)}, u32[]{:S(2)}, u32[]{:S(2)}) collective-permute-start(bf16[32,2048]{1,0:T(8,128)(2,1)S(1)} %collective-permute-done.21), channel_id=1, source_target_pairs={{0,8},{1,17},{2,10},{3,19},{4,12},{5,21},{6,14},{7,23},{8,0},{9,25... | collective-permute-start | bytes 393224 | tf_op jit(solution)/shard_map/ppermute | solution.py:56
  45.8 8.1 %collective-permute-start.16 = (bf16[32,2048]{1,0:T(8,128)(2,1)S(1)}, bf16[32,2048]{1,0:T(8,128)(2,1)S(1)}, u32[]{:S(2)}, u32[]{:S(2)}) collective-permute-start(bf16[32,2048]{1,0:T(8,128)(2,1)S(1)} %collective-permute-done.15), channel_id=1, source_target_pairs={{0,8},{1,17},{2,10},{3,19},{4,12},{5,21},{6,14},{7,23},{8,0},{9,25... | collective-permute-start | bytes 393224 | tf_op jit(solution)/shard_map/ppermute | solution.py:56
  48.6 6.4 %collective-permute-start.29 = (bf16[64,2048]{1,0:T(8,128)(2,1)S(1)}, bf16[64,2048]{1,0:T(8,128)(2,1)S(1)}, u32[]{:S(2)}, u32[]{:S(2)}) collective-permute-start(bf16[64,2048]{1,0:T(8,128)(2,1)S(1)} %constant_dynamic-update-slice_fusion.6.refs_0_), channel_id=1, source_target_pairs={{0,16},{1,9},{2,18},{3,11},{4,20},{5,13},{6,22},{7,15},{8,24},{9,1... | collective-permute-start | bytes 786440 | tf_op jit(solution)/shard_map/ppermute | solution.py:56
  51.1 9.3 %collective-permute-start.23 = (bf16[64,2048]{1,0:T(8,128)(2,1)S(1)}, bf16[64,2048]{1,0:T(8,128)(2,1)S(1)}, u32[]{:S(2)}, u32[]{:S(2)}) collective-permute-start(bf16[64,2048]{1,0:T(8,128)(2,1)S(1)} %constant_dynamic-update-slice_fusion.4.refs_0_), channel_id=1, source_target_pairs={{0,16},{1,9},{2,18},{3,11},{4,20},{5,13},{6,22},{7,15},{8,24},{9,1... | collective-permute-start | bytes 786440 | tf_op jit(solution)/shard_map/ppermute | solution.py:56
  53.9 10.5 %collective-permute-start.17 = (bf16[64,2048]{1,0:T(8,128)(2,1)S(1)}, bf16[64,2048]{1,0:T(8,128)(2,1)S(1)}, u32[]{:S(2)}, u32[]{:S(2)}) collective-permute-start(bf16[64,2048]{1,0:T(8,128)(2,1)S(1)} %constant_dynamic-update-slice_fusion.2.refs_0_), channel_id=1, source_target_pairs={{0,16},{1,9},{2,18},{3,11},{4,20},{5,13},{6,22},{7,15},{8,24},{9,1... | collective-permute-start | bytes 786440 | tf_op jit(solution)/shard_map/ppermute | solution.py:56
  55.0 13.5 %collective-permute-start.10 = (bf16[64,2048]{1,0:T(8,128)(2,1)S(1)}, bf16[64,2048]{1,0:T(8,128)(2,1)S(1)}, u32[]{:S(2)}, u32[]{:S(2)}) collective-permute-start(bf16[64,2048]{1,0:T(8,128)(2,1)S(1)} %constant_dynamic-update-slice_fusion.refs_0_), channel_id=1, source_target_pairs={{0,16},{1,9},{2,18},{3,11},{4,20},{5,13},{6,22},{7,15},{8,24},{9,1... | collective-permute-start | bytes 786440 | tf_op jit(solution)/shard_map/ppermute | solution.py:56
  59.2 13.3 %collective-permute-start.30 = (bf16[64,2048]{1,0:T(8,128)(2,1)S(1)}, bf16[64,2048]{1,0:T(8,128)(2,1)S(1)}, u32[]{:S(2)}, u32[]{:S(2)}) collective-permute-start(bf16[64,2048]{1,0:T(8,128)(2,1)S(1)} %get-tuple-element.82), channel_id=1, source_target_pairs={{0,16},{1,9},{2,18},{3,11},{4,20},{5,13},{6,22},{7,15},{8,24},{9,1... | collective-permute-start | bytes 786440 | tf_op jit(solution)/shard_map/ppermute | solution.py:56
  63.3 10.1 %collective-permute-start.24 = (bf16[64,2048]{1,0:T(8,128)(2,1)S(1)}, bf16[64,2048]{1,0:T(8,128)(2,1)S(1)}, u32[]{:S(2)}, u32[]{:S(2)}) collective-permute-start(bf16[64,2048]{1,0:T(8,128)(2,1)S(1)} %get-tuple-element.80), channel_id=1, source_target_pairs={{0,16},{1,9},{2,18},{3,11},{4,20},{5,13},{6,22},{7,15},{8,24},{9,1... | collective-permute-start | bytes 786440 | tf_op jit(solution)/shard_map/ppermute | solution.py:56
  67.4 7.4 %collective-permute-start.18 = (bf16[64,2048]{1,0:T(8,128)(2,1)S(1)}, bf16[64,2048]{1,0:T(8,128)(2,1)S(1)}, u32[]{:S(2)}, u32[]{:S(2)}) collective-permute-start(bf16[64,2048]{1,0:T(8,128)(2,1)S(1)} %get-tuple-element.78), channel_id=1, source_target_pairs={{0,16},{1,9},{2,18},{3,11},{4,20},{5,13},{6,22},{7,15},{8,24},{9,1... | collective-permute-start | bytes 786440 | tf_op jit(solution)/shard_map/ppermute | solution.py:56
  71.5 9.2 %collective-permute-start.13 = (bf16[64,2048]{1,0:T(8,128)(2,1)S(1)}, bf16[64,2048]{1,0:T(8,128)(2,1)S(1)}, u32[]{:S(2)}, u32[]{:S(2)}) collective-permute-start(bf16[64,2048]{1,0:T(8,128)(2,1)S(1)} %get-tuple-element.76), channel_id=1, source_target_pairs={{0,16},{1,9},{2,18},{3,11},{4,20},{5,13},{6,22},{7,15},{8,24},{9,1... | collective-permute-start | bytes 786440 | tf_op jit(solution)/shard_map/ppermute | solution.py:56
  72.6 8.9 %collective-permute-start.31 = (bf16[32,2048]{1,0:T(8,128)(2,1)S(1)}, bf16[32,2048]{1,0:T(8,128)(2,1)S(1)}, u32[]{:S(2)}, u32[]{:S(2)}) collective-permute-start(bf16[32,2048]{1,0:T(8,128)(2,1)S(1)} %add_convert_fusion.2), channel_id=1, source_target_pairs={{0,8},{1,17},{2,10},{3,19},{4,12},{5,21},{6,14},{7,23},{8,0},{9,25... | collective-permute-start | bytes 393224 | tf_op jit(solution)/shard_map/ppermute | solution.py:56
  73.5 9.9 %collective-permute-start.25 = (bf16[32,2048]{1,0:T(8,128)(2,1)S(1)}, bf16[32,2048]{1,0:T(8,128)(2,1)S(1)}, u32[]{:S(2)}, u32[]{:S(2)}) collective-permute-start(bf16[32,2048]{1,0:T(8,128)(2,1)S(1)} %add_convert_fusion.4), channel_id=1, source_target_pairs={{0,8},{1,17},{2,10},{3,19},{4,12},{5,21},{6,14},{7,23},{8,0},{9,25... | collective-permute-start | bytes 393224 | tf_op jit(solution)/shard_map/ppermute | solution.py:56
  74.8 10.3 %collective-permute-start.19 = (bf16[32,2048]{1,0:T(8,128)(2,1)S(1)}, bf16[32,2048]{1,0:T(8,128)(2,1)S(1)}, u32[]{:S(2)}, u32[]{:S(2)}) collective-permute-start(bf16[32,2048]{1,0:T(8,128)(2,1)S(1)} %add_convert_fusion.6), channel_id=1, source_target_pairs={{0,8},{1,17},{2,10},{3,19},{4,12},{5,21},{6,14},{7,23},{8,0},{9,25... | collective-permute-start | bytes 393224 | tf_op jit(solution)/shard_map/ppermute | solution.py:56
  80.8 5.4 %collective-permute-start.14 = (bf16[32,2048]{1,0:T(8,128)(2,1)S(1)}, bf16[32,2048]{1,0:T(8,128)(2,1)S(1)}, u32[]{:S(2)}, u32[]{:S(2)}) collective-permute-start(bf16[32,2048]{1,0:T(8,128)(2,1)S(1)} %add_convert_fusion.8), channel_id=1, source_target_pairs={{0,8},{1,17},{2,10},{3,19},{4,12},{5,21},{6,14},{7,23},{8,0},{9,25... | collective-permute-start | bytes 393224 | tf_op jit(solution)/shard_map/ppermute | solution.py:56
  81.5 6.9 %collective-permute-start.32 = (bf16[32,2048]{1,0:T(8,128)(2,1)S(1)}, bf16[32,2048]{1,0:T(8,128)(2,1)S(1)}, u32[]{:S(2)}, u32[]{:S(2)}) collective-permute-start(bf16[32,2048]{1,0:T(8,128)(2,1)S(1)} %add_convert_fusion.1), channel_id=1, source_target_pairs={{0,6},{1,7},{2,4},{3,5},{4,2},{5,3},{6,0},{7,1},{8,14},{9,15},{10,... | collective-permute-start | bytes 393224 | tf_op jit(solution)/shard_map/ppermute | solution.py:46
  83.4 8.7 %collective-permute-start.26 = (bf16[32,2048]{1,0:T(8,128)(2,1)S(1)}, bf16[32,2048]{1,0:T(8,128)(2,1)S(1)}, u32[]{:S(2)}, u32[]{:S(2)}) collective-permute-start(bf16[32,2048]{1,0:T(8,128)(2,1)S(1)} %add_convert_fusion.3), channel_id=1, source_target_pairs={{0,4},{1,5},{2,6},{3,7},{4,0},{5,1},{6,2},{7,3},{8,12},{9,13},{10,... | collective-permute-start | bytes 393224 | tf_op jit(solution)/shard_map/ppermute | solution.py:46
  85.1 7.0 %collective-permute-start.20 = (bf16[32,2048]{1,0:T(8,128)(2,1)S(1)}, bf16[32,2048]{1,0:T(8,128)(2,1)S(1)}, u32[]{:S(2)}, u32[]{:S(2)}) collective-permute-start(bf16[32,2048]{1,0:T(8,128)(2,1)S(1)} %add_convert_fusion.5), channel_id=1, source_target_pairs={{0,2},{1,3},{2,0},{3,1},{4,6},{5,7},{6,4},{7,5},{8,10},{9,11},{10,... | collective-permute-start | bytes 393224 | tf_op jit(solution)/shard_map/ppermute | solution.py:46
where the time goes:
time: 93 us; the launch traced here: 92.9 us
  waiting for transfers between devices  41.8 us (45%)
  starting transfers between devices  33.4 us (36%)
  Pallas kernels  16.3 us (18%)
  other arithmetic  1.07 us (1%)
    ppermute x17, waiting for transfers between devices, flip(): lax.ppermute(value, axis, [(i, i ^ distance) for i in range(lax.axis_size...  29.9 us
    ppermute x17, starting transfers between devices, flip(): lax.ppermute(value, axis, [(i, i ^ distance) for i in range(lax.axis_size...  19.4 us
    pallas_call x9, Pallas kernels, vmem_call(): pl.pallas_call(kernel, in_specs=[far] * len(far_args) + [near] * len(args...  16.3 us
    ppermute x16, starting transfers between devices, flip_plane(): return lax.ppermute(value, ('sp', 'tp'), pairs)  14 us
    ppermute x16, waiting for transfers between devices, flip_plane(): return lax.ppermute(value, ('sp', 'tp'), pairs)  11.9 us
  transfers between devices with their start and end apart: 33, of which 15 were waited for; matrix products, arithmetic and copies ran while one was open for 0% of the time, Pallas kernels for 17%

commit v1 on v0

--- a/solution.py
+++ b/solution.py
@@ -126,17 +126,16 @@
 
 
 def lru_kernel(*refs):
-    far, refs = refs[:13], refs[13:]
+    far, refs = refs[:12], refs[12:]
     (state_out, run_out, mix_out), refs = refs[:3], refs[3:]
     messages, refs = refs[:PLANE], refs[PLANE:]
-    (taps, rate_w, inlet_w, decay_in, out_w, residual, down_w), refs = refs[:7], refs[7:]
+    (taps, rate_w, inlet_w, decay_in, out_w, residual), refs = refs[:6], refs[6:]
     rows_in, gate_in, docs, gain, routes, route_w, padded, doc_cols, sems = refs
     block = residual.shape[0]
     own = pl.ds(pl.multiple_of(lax.axis_index("tp") * block, block), block)
-    sources = [*far[:11], far[11].at[own], far[12]]
+    sources = [*far[:11], far[11].at[own]]
     targets = (
         rows_in, docs, taps, rate_w, inlet_w, decay_in, gate_in, gain, routes, route_w, out_w, residual,
-        down_w,
     )
     copies = [
         pltpu.make_async_copy(source, target, sems.at[i])
@@ -144,7 +143,7 @@
     ]
     for copy in copies:
         copy.start()
-    for copy in copies[:-3]:
+    for copy in copies[:-2]:
         copy.wait()
     positions, channels = rows_in.shape
     reach = taps.shape[0] - 1
@@ -181,7 +180,21 @@
         message[2:3, 0:positions] = dense
         message[EDGE, 0:channels] = ends(padded)
         message[EDGE_DOCS, 0:LANES] = ends(doc_cols)
-    for copy in copies[-3:]:
+    for copy in copies[-2:]:
+        copy.wait()
+
+
+def fetch_kernel(far, near, sems):
+    count = sems.shape[0]
+    rows = far.shape[0] // count
+    pieces = [pl.ds(i * rows, rows) for i in range(count)]
+    copies = [
+        pltpu.make_async_copy(far.at[piece], near.at[piece], sems.at[i])
+        for i, piece in enumerate(pieces)
+    ]
+    for copy in copies:
+        copy.start()
+    for copy in copies:
         copy.wait()
 
 
@@ -394,7 +407,6 @@
         + [
             (conv_taps.shape, BF16), (rate_weight.shape, BF16), (inlet_weight.shape, BF16),
             ((1, channels), F32), (out_weight.shape, BF16), ((block, width), BF16),
-            (w_down.shape[1:], BF16),
         ],
         [],
         scratch=[
@@ -406,19 +418,18 @@
             (routes.T.shape, F32),
             ((SUBLANES + positions, channels), F32),
             ((SUBLANES + positions, LANES), F32),
-            pltpu.SemaphoreType.DMA((13,)),
+            pltpu.SemaphoreType.DMA((12,)),
         ],
         far_args=[
             lru_input, documents[None, :], conv_taps, rate_weight, inlet_weight,
             decay_param[None, :], gate_input, lru_gain[None, :], routes.T, route_weights.T,
-            out_weight, residual, w_down[0],
+            out_weight, residual,
         ],
     )
     messages, params = rest[:PLANE], rest[PLANE:]
-    taps, rate_w, inlet_w, decay_in, own_out, own_residual, own_down = params
+    taps, rate_w, inlet_w, decay_in, own_out, own_residual = params
     messages = [messages[0]] + [flip(messages[k], "sp", k) for k in range(1, PLANE)]
-    early = flip(w_gate[0], "tp", 1)
-    messages, other_out, early = lax.optimization_barrier((messages, other_out, early))
+    messages, other_out = lax.optimization_barrier((messages, other_out))
 
     half_rows = positions // CORES
     packed = (half_rows, channels + LANES)
@@ -436,13 +447,20 @@
             ((positions, channels + LANES), BF16),
         ],
     )
-    other, *own = lax.optimization_barrier((flip(send, "tp", 1), w_up[0], w_down[0]))
-    swapped = [early] + [flip(value, "tp", 1) for value in own]
+    other, *own = lax.optimization_barrier((flip(send, "tp", 1), w_gate[0], w_up[0], w_down[0]))
+    swapped = [flip(value, "tp", 1) for value in own]
     parts = vmem_call(
         functools.partial(project_kernel, block=block),
         [((block, width + LANES), BF16)] * depths,
         [keep, other, own_out, other_out],
         scratch=[(packed, BF16)] * 2,
+    )
+    [own_down] = vmem_call(
+        fetch_kernel,
+        [(w_down.shape[1:], BF16)],
+        [],
+        scratch=[pltpu.SemaphoreType.DMA((4,))],
+        far_args=[w_down[0]],
     )
     parts = dict(enumerate(parts))
     for k in range(depths - 1, 1, -1):

time: 93 us -> 101 us (1.086)
  waiting for transfers between devices: 41.8 us -> 48.5 us
  Pallas kernels: 16.3 us -> 18 us
    ppermute x16, waiting for transfers between devices: 11.9 us -> 22 us  [flip_plane(): return lax.ppermute(value, ('sp', 'tp'), pairs)]
    ppermute x17, waiting for transfers between devices: 29.9 us -> 26.5 us  [flip(): lax.ppermute(value, axis, [(i, i ^ distance) for i in range(lax.axis_size...]
    ppermute x17, starting transfers between devices: 19.4 us -> 22.2 us  [flip(): lax.ppermute(value, axis, [(i, i ^ distance) for i in range(lax.axis_size...]
    ppermute x16, starting transfers between devices: 14 us -> 11.2 us  [flip_plane(): return lax.ppermute(value, ('sp', 'tp'), pairs)]
    pallas_call x9 -> x10, Pallas kernels: 16.3 us -> 18 us  [vmem_call(): pl.pallas_call(kernel, in_specs=[far] * len(far_args) + [near] * len(args...]
  transfers between devices with their start and end apart: 33 -> 33, of which waited for: 15 -> 18; matrix products, arithmetic and copies ran while one was open for 0% -> 0% of each run, Pallas kernels for 17% -> 17%
where the time goes in v1:
time: 101 us
  waiting for transfers between devices  48.5 us (48%)
  starting transfers between devices  33.5 us (33%)
  Pallas kernels  18 us (18%)
  other arithmetic  1.07 us (1%)
    ppermute x17, waiting for transfers between devices, flip(): lax.ppermute(value, axis, [(i, i ^ distance) for i in range(lax.axis_size...  26.5 us
    ppermute x17, starting transfers between devices, flip(): lax.ppermute(value, axis, [(i, i ^ distance) for i in range(lax.axis_size...  22.2 us
    ppermute x16, waiting for transfers between devices, flip_plane(): return lax.ppermute(value, ('sp', 'tp'), pairs)  22 us
    pallas_call x10, Pallas kernels, vmem_call(): pl.pallas_call(kernel, in_specs=[far] * len(far_args) + [near] * len(args...  18 us
    ppermute x16, starting transfers between devices, flip_plane(): return lax.ppermute(value, ('sp', 'tp'), pairs)  11.2 us
  transfers between devices with their start and end apart: 33, of which 18 were waited for; matrix products, arithmetic and copies ran while one was open for 0% of the time, Pallas kernels for 17%

profile of v1, /device:TPU:0, one launch (start us, length us, event | category | flops | bytes accessed | tf_op | source)
XLA Modules:
  0.0 101.3 jit_solution(17812014345979356790)
XLA Ops:
  0.0 0.5 collective-permute-start.3
  0.5 2.5 %shard_map.154 = (f32[256,256]{1,0:T(8,128)S(1)}, f32[256,256]{1,0:T(8,128)S(1)}, f32[256,256]{1,0:T(8,128)S(1)}, f32[24,256]{1,0:T(8,128)S(1)}, f32[24,256]{1,0...) custom-call(bf16[256,256]{1,0:T(8,128)(2,1)} %refs_0_.1, ...), custom_call_target="tpu_custom_call" | custom-call | tf_op jit(solution)/shard_map/pallas_call | solution.py:25
  3.0 2.5 %collective-permute-start = (f32[24,256]{1,0:T(8,128)S(1)}, f32[24,256]{1,0:T(8,128)S(1)}, u32[]{:S(2)}, u32[]{:S(2)}) collective-permute-start(f32[24,256]{1,0:T(8,128)S(1)} %get-tuple-element.52), channel_id=1, source_target_pairs={{0,8},{8,0},{16,24},{24,16},{1,9},{9,1},{17,25},{25,17},{2,10},{10... | collective-permute-start | bytes 73736 | tf_op jit(solution)/shard_map/ppermute | solution.py:46
  5.5 1.5 %collective-permute-start.1 = (f32[24,256]{1,0:T(8,128)S(1)}, f32[24,256]{1,0:T(8,128)S(1)}, u32[]{:S(2)}, u32[]{:S(2)}) collective-permute-start(f32[24,256]{1,0:T(8,128)S(1)} %get-tuple-element.53), channel_id=1, source_target_pairs={{0,16},{8,24},{16,0},{24,8},{1,17},{9,25},{17,1},{25,9},{2,18},{10... | collective-permute-start | bytes 73736 | tf_op jit(solution)/shard_map/ppermute | solution.py:46
  7.5 1.8 %collective-permute-done.1.rest_2_.refs_4_ = f32[24,256]{1,0:T(8,128)S(1)} collective-permute-done((f32[24,256]{1,0:T(8,128)S(1)}, f32[24,256]{1,0:T(8,128)S(1)}, u32[]{:S(2)}, u32[]{:S(2)}) %collective-permute-start.1) | collective-permute-done | bytes 24608 | tf_op jit(solution)/shard_map/ppermute | solution.py:46
  9.3 2.4 %collective-permute-done.2.rest_3_.refs_5_ = f32[24,256]{1,0:T(8,128)S(1)} collective-permute-done((f32[24,256]{1,0:T(8,128)S(1)}, f32[24,256]{1,0:T(8,128)S(1)}, u32[]{:S(2)}, u32[]{:S(2)}) %collective-permute-start.2) | collective-permute-done | bytes 24608 | tf_op jit(solution)/shard_map/ppermute | solution.py:46
  12.2 1.3 %collective-permute-done.4.other = bf16[128,384]{1,0:T(8,128)(2,1)S(1)} collective-permute-done((bf16[128,384]{1,0:T(8,128)(2,1)S(1)}, bf16[128,384]{1,0:T(8,128)(2,1)S(1)}, u32[]{:S(2)}, u32[]{:S(2)}) %collective-permute-start.4) | collective-permute-done | bytes 98336 | tf_op jit(solution)/shard_map/ppermute | solution.py:46
  14.7 1.6 %collective-permute-start.6 = (bf16[32,2176]{1,0:T(8,128)(2,1)S(1)}, bf16[32,2176]{1,0:T(8,128)(2,1)S(1)}, u32[]{:S(2)}, u32[]{:S(2)}) collective-permute-start(bf16[32,2176]{1,0:T(8,128)(2,1)S(1)} %get-tuple-element.67), channel_id=1, source_target_pairs={{0,2},{1,3},{2,0},{3,1},{4,6},{5,7},{6,4},{7,5},{8,10},{9,11},{10,... | collective-permute-start | bytes 417800 | tf_op jit(solution)/shard_map/ppermute | solution.py:46
  16.8 4.5 %collective-permute-done.6.two = bf16[32,2176]{1,0:T(8,128)(2,1)S(1)} collective-permute-done((bf16[32,2176]{1,0:T(8,128)(2,1)S(1)}, bf16[32,2176]{1,0:T(8,128)(2,1)S(1)}, u32[]{:S(2)}, u32[]{:S(2)}) %collective-permute-start.6) | collective-permute-done | bytes 139296 | tf_op jit(solution)/shard_map/ppermute | solution.py:46
  21.5 2.6 %collective-permute-start.7 = (bf16[32,2176]{1,0:T(8,128)(2,1)S(1)}, bf16[32,2176]{1,0:T(8,128)(2,1)S(1)}, u32[]{:S(2)}, u32[]{:S(2)}) collective-permute-start(bf16[32,2176]{1,0:T(8,128)(2,1)S(1)} %shard_map.157), channel_id=1, source_target_pairs={{0,4},{1,5},{2,6},{3,7},{4,0},{5,1},{6,2},{7,3},{8,12},{9,13},{10,... | collective-permute-start | bytes 417800 | tf_op jit(solution)/shard_map/ppermute | solution.py:46
  24.1 1.9 %shard_map.159.refs_10_ = bf16[768,2048]{1,0:T(8,128)(2,1)S(1)} custom-call(bf16[768,2048]{1,0:T(8,128)(2,1)} %bitcast.21), custom_call_target="tpu_custom_call" | custom-call | tf_op jit(solution)/shard_map/pallas_call | solution.py:25
  26.0 4.0 %collective-permute-done.7.rest_2_ = bf16[32,2176]{1,0:T(8,128)(2,1)S(1)} collective-permute-done((bf16[32,2176]{1,0:T(8,128)(2,1)S(1)}, bf16[32,2176]{1,0:T(8,128)(2,1)S(1)}, u32[]{:S(2)}, u32[]{:S(2)}) %collective-permute-start.7) | collective-permute-done | bytes 139296 | tf_op jit(solution)/shard_map/ppermute | solution.py:46
  30.3 3.4 %collective-permute-start.27 = (bf16[32,2048]{1,0:T(8,128)(2,1)S(1)}, bf16[32,2048]{1,0:T(8,128)(2,1)S(1)}, u32[]{:S(2)}, u32[]{:S(2)}) collective-permute-start(bf16[32,2048]{1,0:T(8,128)(2,1)S(1)} %get-tuple-element.69), channel_id=1, source_target_pairs={{0,6},{1,7},{2,4},{3,5},{4,2},{5,3},{6,0},{7,1},{8,14},{9,15},{10,... | collective-permute-start | bytes 393224 | tf_op jit(solution)/shard_map/ppermute | solution.py:46
  33.8 4.7 %collective-permute-done.27 = bf16[32,2048]{1,0:T(8,128)(2,1)S(1)} collective-permute-done((bf16[32,2048]{1,0:T(8,128)(2,1)S(1)}, bf16[32,2048]{1,0:T(8,128)(2,1)S(1)}, u32[]{:S(2)}, u32[]{:S(2)}) %collective-permute-start.27) | collective-permute-done | bytes 131104 | tf_op jit(solution)/shard_map/ppermute | solution.py:46
  38.5 4.2 %collective-permute-start.15 = (bf16[32,2048]{1,0:T(8,128)(2,1)S(1)}, bf16[32,2048]{1,0:T(8,128)(2,1)S(1)}, u32[]{:S(2)}, u32[]{:S(2)}) collective-permute-start(bf16[32,2048]{1,0:T(8,128)(2,1)S(1)} %get-tuple-element.69), channel_id=1, source_target_pairs={{0,2},{1,3},{2,0},{3,1},{4,6},{5,7},{6,4},{7,5},{8,10},{9,11},{10,... | collective-permute-start | bytes 393224 | tf_op jit(solution)/shard_map/ppermute | solution.py:46
  42.7 1.0 %collective-permute-done.21 = bf16[32,2048]{1,0:T(8,128)(2,1)S(1)} collective-permute-done((bf16[32,2048]{1,0:T(8,128)(2,1)S(1)}, bf16[32,2048]{1,0:T(8,128)(2,1)S(1)}, u32[]{:S(2)}, u32[]{:S(2)}) %collective-permute-start.21) | collective-permute-done | bytes 131104 | tf_op jit(solution)/shard_map/ppermute | solution.py:46
  43.8 0.5 collective-permute-start.28
  44.3 1.3 %collective-permute-done.15 = bf16[32,2048]{1,0:T(8,128)(2,1)S(1)} collective-permute-done((bf16[32,2048]{1,0:T(8,128)(2,1)S(1)}, bf16[32,2048]{1,0:T(8,128)(2,1)S(1)}, u32[]{:S(2)}, u32[]{:S(2)}) %collective-permute-start.15) | collective-permute-done | bytes 131104 | tf_op jit(solution)/shard_map/ppermute | solution.py:46
  45.7 0.5 collective-permute-start.22
  46.2 2.5 %collective-permute-done.28 = bf16[32,2048]{1,0:T(8,128)(2,1)S(1)} collective-permute-done((bf16[32,2048]{1,0:T(8,128)(2,1)S(1)}, bf16[32,2048]{1,0:T(8,128)(2,1)S(1)}, u32[]{:S(2)}, u32[]{:S(2)}) %collective-permute-start.28) | collective-permute-done | bytes 131104 | tf_op jit(solution)/shard_map/ppermute | solution.py:56
  48.7 0.5 collective-permute-start.16
  49.3 1.3 %collective-permute-done.22 = bf16[32,2048]{1,0:T(8,128)(2,1)S(1)} collective-permute-done((bf16[32,2048]{1,0:T(8,128)(2,1)S(1)}, bf16[32,2048]{1,0:T(8,128)(2,1)S(1)}, u32[]{:S(2)}, u32[]{:S(2)}) %collective-permute-start.22) | collective-permute-done | bytes 131104 | tf_op jit(solution)/shard_map/ppermute | solution.py:56
  50.6 0.5 collective-permute-start.29
  51.2 3.9 %collective-permute-done.16 = bf16[32,2048]{1,0:T(8,128)(2,1)S(1)} collective-permute-done((bf16[32,2048]{1,0:T(8,128)(2,1)S(1)}, bf16[32,2048]{1,0:T(8,128)(2,1)S(1)}, u32[]{:S(2)}, u32[]{:S(2)}) %collective-permute-start.16) | collective-permute-done | bytes 131104 | tf_op jit(solution)/shard_map/ppermute | solution.py:56
  55.0 0.5 collective-permute-start.8
  55.6 5.8 %collective-permute-done.8 = bf16[32,2048]{1,0:T(8,128)(2,1)S(1)} collective-permute-done((bf16[32,2048]{1,0:T(8,128)(2,1)S(1)}, bf16[32,2048]{1,0:T(8,128)(2,1)S(1)}, u32[]{:S(2)}, u32[]{:S(2)}) %collective-permute-start.8) | collective-permute-done | bytes 131104 | tf_op jit(solution)/shard_map/ppermute | solution.py:56
  61.4 0.5 collective-permute-start.23
  61.9 1.5 %collective-permute-start.17 = (bf16[64,2048]{1,0:T(8,128)(2,1)S(1)}, bf16[64,2048]{1,0:T(8,128)(2,1)S(1)}, u32[]{:S(2)}, u32[]{:S(2)}) collective-permute-start(bf16[64,2048]{1,0:T(8,128)(2,1)S(1)} %constant_dynamic-update-slice_fusion.2.refs_0_), channel_id=1, source_target_pairs={{0,16},{1,9},{2,18},{3,11},{4,20},{5,13},{6,22},{7,15},{8,24},{9,1... | collective-permute-start | bytes 786440 | tf_op jit(solution)/shard_map/ppermute | solution.py:56
  63.4 0.6 collective-permute-start.9
  64.0 3.2 %shard_map.163 = (bf16[64,2048]{1,0:T(8,128)(2,1)S(1)}, bf16[64,2048]{1,0:T(8,128)(2,1)S(1)}) custom-call(bf16[64,2048]{1,0:T(8,128)(2,1)S(1)} %constant_dynamic-update-slice_fusion.6.refs_0_, bf16[64,2048]{1,0:T(8,128)(2,1)S(1)} %collective-permute-done.29.refs_1_, f32[24,256]{1,0:T(8,128)S(1)} %get-tuple-element.55.rest_0_.refs_2_, ...), custom_call_target="tpu_custom_call" | custom-call | tf_op jit(solution)/shard_map/pallas_call | solution.py:25
  67.2 1.6 %collective-permute-start.30 = (bf16[64,2048]{1,0:T(8,128)(2,1)S(1)}, bf16[64,2048]{1,0:T(8,128)(2,1)S(1)}, u32[]{:S(2)}, u32[]{:S(2)}) collective-permute-start(bf16[64,2048]{1,0:T(8,128)(2,1)S(1)} %get-tuple-element.80), channel_id=1, source_target_pairs={{0,16},{1,9},{2,18},{3,11},{4,20},{5,13},{6,22},{7,15},{8,24},{9,1... | collective-permute-start | bytes 786440 | tf_op jit(solution)/shard_map/ppermute | solution.py:56
  68.8 3.0 %shard_map.162 = (bf16[64,2048]{1,0:T(8,128)(2,1)S(1)}, bf16[64,2048]{1,0:T(8,128)(2,1)S(1)}) custom-call(bf16[64,2048]{1,0:T(8,128)(2,1)S(1)} %constant_dynamic-update-slice_fusion.4.refs_0_, bf16[64,2048]{1,0:T(8,128)(2,1)S(1)} %collective-permute-done.23.refs_1_, f32[24,256]{1,0:T(8,128)S(1)} %get-tuple-element.55.rest_0_.refs_2_, ...), custom_call_target="tpu_custom_call" | custom-call | tf_op jit(solution)/shard_map/pallas_call | solution.py:25
  71.8 0.6 collective-permute-start.24
  72.4 3.0 %shard_map.161 = (bf16[64,2048]{1,0:T(8,128)(2,1)S(1)}, bf16[64,2048]{1,0:T(8,128)(2,1)S(1)}) custom-call(bf16[64,2048]{1,0:T(8,128)(2,1)S(1)} %constant_dynamic-update-slice_fusion.2.refs_0_, bf16[64,2048]{1,0:T(8,128)(2,1)S(1)} %collective-permute-done.17.refs_1_, f32[24,256]{1,0:T(8,128)S(1)} %get-tuple-element.55.rest_0_.refs_2_, ...), custom_call_target="tpu_custom_call" | custom-call | tf_op jit(solution)/shard_map/pallas_call | solution.py:25
  75.4 1.6 %collective-permute-start.18 = (bf16[64,2048]{1,0:T(8,128)(2,1)S(1)}, bf16[64,2048]{1,0:T(8,128)(2,1)S(1)}, u32[]{:S(2)}, u32[]{:S(2)}) collective-permute-start(bf16[64,2048]{1,0:T(8,128)(2,1)S(1)} %get-tuple-element.76), channel_id=1, source_target_pairs={{0,16},{1,9},{2,18},{3,11},{4,20},{5,13},{6,22},{7,15},{8,24},{9,1... | collective-permute-start | bytes 786440 | tf_op jit(solution)/shard_map/ppermute | solution.py:56
  77.0 3.0 %shard_map.160 = (bf16[64,2048]{1,0:T(8,128)(2,1)S(1)}, bf16[64,2048]{1,0:T(8,128)(2,1)S(1)}) custom-call(bf16[64,2048]{1,0:T(8,128)(2,1)S(1)} %constant_dynamic-update-slice_fusion.refs_0_, bf16[64,2048]{1,0:T(8,128)(2,1)S(1)} %collective-permute-done.9.refs_1_, f32[24,256]{1,0:T(8,128)S(1)} %get-tuple-element.55.rest_0_.refs_2_, ...), custom_call_target="tpu_custom_call" | custom-call | tf_op jit(solution)/shard_map/pallas_call | solution.py:25
  80.0 0.6 collective-permute-start.13
  80.6 0.6 collective-permute-start.31
  81.2 1.4 %collective-permute-done.24 = bf16[64,2048]{1,0:T(8,128)(2,1)S(1)} collective-permute-done((bf16[64,2048]{1,0:T(8,128)(2,1)S(1)}, bf16[64,2048]{1,0:T(8,128)(2,1)S(1)}, u32[]{:S(2)}, u32[]{:S(2)}) %collective-permute-start.24) | collective-permute-done | bytes 262176 | tf_op jit(solution)/shard_map/ppermute | solution.py:56
  82.8 4.6 %collective-permute-done.18 = bf16[64,2048]{1,0:T(8,128)(2,1)S(1)} collective-permute-done((bf16[64,2048]{1,0:T(8,128)(2,1)S(1)}, bf16[64,2048]{1,0:T(8,128)(2,1)S(1)}, u32[]{:S(2)}, u32[]{:S(2)}) %collective-permute-start.18) | collective-permute-done | bytes 262176 | tf_op jit(solution)/shard_map/ppermute | solution.py:56
  87.8 2.4 %collective-permute-done.13 = bf16[64,2048]{1,0:T(8,128)(2,1)S(1)} collective-permute-done((bf16[64,2048]{1,0:T(8,128)(2,1)S(1)}, bf16[64,2048]{1,0:T(8,128)(2,1)S(1)}, u32[]{:S(2)}, u32[]{:S(2)}) %collective-permute-start.13) | collective-permute-done | bytes 262176 | tf_op jit(solution)/shard_map/ppermute | solution.py:56
  90.3 0.6 collective-permute-start.14
  90.9 1.3 %collective-permute-start.32 = (bf16[32,2048]{1,0:T(8,128)(2,1)S(1)}, bf16[32,2048]{1,0:T(8,128)(2,1)S(1)}, u32[]{:S(2)}, u32[]{:S(2)}) collective-permute-start(bf16[32,2048]{1,0:T(8,128)(2,1)S(1)} %add_convert_fusion.1), channel_id=1, source_target_pairs={{0,6},{1,7},{2,4},{3,5},{4,2},{5,3},{6,0},{7,1},{8,14},{9,15},{10,... | collective-permute-start | bytes 393224 | tf_op jit(solution)/shard_map/ppermute | solution.py:46
  92.3 0.7 collective-permute-start.26
  93.0 2.6 %collective-permute-start.20 = (bf16[32,2048]{1,0:T(8,128)(2,1)S(1)}, bf16[32,2048]{1,0:T(8,128)(2,1)S(1)}, u32[]{:S(2)}, u32[]{:S(2)}) collective-permute-start(bf16[32,2048]{1,0:T(8,128)(2,1)S(1)} %add_convert_fusion.5), channel_id=1, source_target_pairs={{0,2},{1,3},{2,0},{3,1},{4,6},{5,7},{6,4},{7,5},{8,10},{9,11},{10,... | collective-permute-start | bytes 393224 | tf_op jit(solution)/shard_map/ppermute | solution.py:46
  95.6 2.3 %collective-permute-done.32 = bf16[32,2048]{1,0:T(8,128)(2,1)S(1)} collective-permute-done((bf16[32,2048]{1,0:T(8,128)(2,1)S(1)}, bf16[32,2048]{1,0:T(8,128)(2,1)S(1)}, u32[]{:S(2)}, u32[]{:S(2)}) %collective-permute-start.32) | collective-permute-done | bytes 131104 | tf_op jit(solution)/shard_map/ppermute | solution.py:46
  97.9 2.6 %collective-permute-done.26 = bf16[32,2048]{1,0:T(8,128)(2,1)S(1)} collective-permute-done((bf16[32,2048]{1,0:T(8,128)(2,1)S(1)}, bf16[32,2048]{1,0:T(8,128)(2,1)S(1)}, u32[]{:S(2)}, u32[]{:S(2)}) %collective-permute-start.26) | collective-permute-done | bytes 131104 | tf_op jit(solution)/shard_map/ppermute | solution.py:46
  100.6 0.8 add_convert_fusion
  (50 shorter events, 4.0 us)
Async XLA Ops:
  0.0 13.5 %copy-start = (bf16[1,2048,768]{2,1,0:T(8,128)(2,1)S(1)}, bf16[1,2048,768]{2,1,0:T(8,128)(2,1)}, u32[]{:S(2)}) copy-start(bf16[1,2048,768]{2,1,0:T(8,128)(2,1)} %param.29) | copy-start | bytes 9437188
  0.0 11.8 %collective-permute-start.3 = (bf16[256,2048]{1,0:T(8,128)(2,1)}, bf16[256,2048]{1,0:T(8,128)(2,1)S(1)}, u32[]{:S(2)}, u32[]{:S(2)}) collective-permute-start(bf16[256,2048]{1,0:T(8,128)(2,1)} %refs_10_.1), channel_id=1, source_target_pairs={{0,1},{1,0},{2,3},{3,2},{4,5},{5,4},{6,7},{7,6},{8,9},{9,8},{10,11... | collective-permute-start | bytes 3145736 | tf_op jit(solution)/shard_map/ppermute | solution.py:46
  3.0 4.5 %collective-permute-start = (f32[24,256]{1,0:T(8,128)S(1)}, f32[24,256]{1,0:T(8,128)S(1)}, u32[]{:S(2)}, u32[]{:S(2)}) collective-permute-start(f32[24,256]{1,0:T(8,128)S(1)} %get-tuple-element.52), channel_id=1, source_target_pairs={{0,8},{8,0},{16,24},{24,16},{1,9},{9,1},{17,25},{25,17},{2,10},{10... | collective-permute-start | bytes 73736 | tf_op jit(solution)/shard_map/ppermute | solution.py:46
  5.5 3.8 %collective-permute-start.1 = (f32[24,256]{1,0:T(8,128)S(1)}, f32[24,256]{1,0:T(8,128)S(1)}, u32[]{:S(2)}, u32[]{:S(2)}) collective-permute-start(f32[24,256]{1,0:T(8,128)S(1)} %get-tuple-element.53), channel_id=1, source_target_pairs={{0,16},{8,24},{16,0},{24,8},{1,17},{9,25},{17,1},{25,9},{2,18},{10... | collective-permute-start | bytes 73736 | tf_op jit(solution)/shard_map/ppermute | solution.py:46
  7.0 4.7 %collective-permute-start.2 = (f32[24,256]{1,0:T(8,128)S(1)}, f32[24,256]{1,0:T(8,128)S(1)}, u32[]{:S(2)}, u32[]{:S(2)}) collective-permute-start(f32[24,256]{1,0:T(8,128)S(1)} %get-tuple-element.54), channel_id=1, source_target_pairs={{0,24},{8,16},{16,8},{24,0},{1,25},{9,17},{17,9},{25,1},{2,26},{10... | collective-permute-start | bytes 73736 | tf_op jit(solution)/shard_map/ppermute | solution.py:46
  12.2 1.4 %collective-permute-start.4 = (bf16[128,384]{1,0:T(8,128)(2,1)S(1)}, bf16[128,384]{1,0:T(8,128)(2,1)S(1)}, u32[]{:S(2)}, u32[]{:S(2)}) collective-permute-start(bf16[128,384]{1,0:T(8,128)(2,1)S(1)} %get-tuple-element.60), channel_id=1, source_target_pairs={{0,1},{1,0},{2,3},{3,2},{4,5},{5,4},{6,7},{7,6},{8,9},{9,8},{10,11... | collective-permute-start | bytes 294920 | tf_op jit(solution)/shard_map/ppermute | solution.py:46
  13.5 49.9 %collective-permute-start.10 = (bf16[2048,768]{1,0:T(8,128)(2,1)S(1)}, bf16[2048,768]{1,0:T(8,128)(2,1)S(1)}, u32[]{:S(2)}, u32[]{:S(2)}) collective-permute-start(bf16[2048,768]{1,0:T(8,128)(2,1)S(1)} %bitcast.9), channel_id=1, source_target_pairs={{0,1},{1,0},{2,3},{3,2},{4,5},{5,4},{6,7},{7,6},{8,9},{9,8},{10,11... | collective-permute-start | bytes 9437192 | tf_op jit(solution)/shard_map/ppermute | solution.py:46
  13.7 50.3 %collective-permute-start.11 = (bf16[2048,768]{1,0:T(8,128)(2,1)}, bf16[2048,768]{1,0:T(8,128)(2,1)S(1)}, u32[]{:S(2)}, u32[]{:S(2)}) collective-permute-start(bf16[2048,768]{1,0:T(8,128)(2,1)} %bitcast.14), channel_id=1, source_target_pairs={{0,1},{1,0},{2,3},{3,2},{4,5},{5,4},{6,7},{7,6},{8,9},{9,8},{10,11... | collective-permute-start | bytes 9437192 | tf_op jit(solution)/shard_map/ppermute | solution.py:46
  14.0 50.0 %collective-permute-start.12 = (bf16[768,2048]{1,0:T(8,128)(2,1)}, bf16[768,2048]{1,0:T(8,128)(2,1)S(1)}, u32[]{:S(2)}, u32[]{:S(2)}) collective-permute-start(bf16[768,2048]{1,0:T(8,128)(2,1)} %bitcast.20), channel_id=1, source_target_pairs={{0,1},{1,0},{2,3},{3,2},{4,5},{5,4},{6,7},{7,6},{8,9},{9,8},{10,11... | collective-permute-start | bytes 9437192 | tf_op jit(solution)/shard_map/ppermute | solution.py:46
  14.7 6.6 %collective-permute-start.6 = (bf16[32,2176]{1,0:T(8,128)(2,1)S(1)}, bf16[32,2176]{1,0:T(8,128)(2,1)S(1)}, u32[]{:S(2)}, u32[]{:S(2)}) collective-permute-start(bf16[32,2176]{1,0:T(8,128)(2,1)S(1)} %get-tuple-element.67), channel_id=1, source_target_pairs={{0,2},{1,3},{2,0},{3,1},{4,6},{5,7},{6,4},{7,5},{8,10},{9,11},{10,... | collective-permute-start | bytes 417800 | tf_op jit(solution)/shard_map/ppermute | solution.py:46
  16.3 9.7 %collective-permute-start.5 = (bf16[32,2176]{1,0:T(8,128)(2,1)S(1)}, bf16[32,2176]{1,0:T(8,128)(2,1)S(1)}, u32[]{:S(2)}, u32[]{:S(2)}) collective-permute-start(bf16[32,2176]{1,0:T(8,128)(2,1)S(1)} %get-tuple-element.65), channel_id=1, source_target_pairs={{0,2},{1,3},{2,0},{3,1},{4,6},{5,7},{6,4},{7,5},{8,10},{9,11},{10,... | collective-permute-start | bytes 417800 | tf_op jit(solution)/shard_map/ppermute | solution.py:46
  21.5 8.5 %copy-start.2 = (f32[2048]{0:T(1024)S(1)}, f32[2048]{0:T(1024)}, u32[]{:S(2)}) copy-start(f32[2048]{0:T(1024)} %param.26) | copy-start | bytes 24580
  21.5 42.5 %copy-start.1 = (bf16[1,2048,768]{2,1,0:T(8,128)(2,1)S(1)}, bf16[1,2048,768]{2,1,0:T(8,128)(2,1)}, u32[]{:S(2)}) copy-start(bf16[1,2048,768]{2,1,0:T(8,128)(2,1)} %param.30) | copy-start | bytes 9437188
  21.5 8.5 %collective-permute-start.7 = (bf16[32,2176]{1,0:T(8,128)(2,1)S(1)}, bf16[32,2176]{1,0:T(8,128)(2,1)S(1)}, u32[]{:S(2)}, u32[]{:S(2)}) collective-permute-start(bf16[32,2176]{1,0:T(8,128)(2,1)S(1)} %shard_map.157), channel_id=1, source_target_pairs={{0,4},{1,5},{2,6},{3,7},{4,0},{5,1},{6,2},{7,3},{8,12},{9,13},{10,... | collective-permute-start | bytes 417800 | tf_op jit(solution)/shard_map/ppermute | solution.py:46
  30.3 8.1 %collective-permute-start.27 = (bf16[32,2048]{1,0:T(8,128)(2,1)S(1)}, bf16[32,2048]{1,0:T(8,128)(2,1)S(1)}, u32[]{:S(2)}, u32[]{:S(2)}) collective-permute-start(bf16[32,2048]{1,0:T(8,128)(2,1)S(1)} %get-tuple-element.69), channel_id=1, source_target_pairs={{0,6},{1,7},{2,4},{3,5},{4,2},{5,3},{6,0},{7,1},{8,14},{9,15},{10,... | collective-permute-start | bytes 393224 | tf_op jit(solution)/shard_map/ppermute | solution.py:46
  33.8 10.0 %collective-permute-start.21 = (bf16[32,2048]{1,0:T(8,128)(2,1)S(1)}, bf16[32,2048]{1,0:T(8,128)(2,1)S(1)}, u32[]{:S(2)}, u32[]{:S(2)}) collective-permute-start(bf16[32,2048]{1,0:T(8,128)(2,1)S(1)} %get-tuple-element.69), channel_id=1, source_target_pairs={{0,4},{1,5},{2,6},{3,7},{4,0},{5,1},{6,2},{7,3},{8,12},{9,13},{10,... | collective-permute-start | bytes 393224 | tf_op jit(solution)/shard_map/ppermute | solution.py:46
  38.5 7.2 %collective-permute-start.15 = (bf16[32,2048]{1,0:T(8,128)(2,1)S(1)}, bf16[32,2048]{1,0:T(8,128)(2,1)S(1)}, u32[]{:S(2)}, u32[]{:S(2)}) collective-permute-start(bf16[32,2048]{1,0:T(8,128)(2,1)S(1)} %get-tuple-element.69), channel_id=1, source_target_pairs={{0,2},{1,3},{2,0},{3,1},{4,6},{5,7},{6,4},{7,5},{8,10},{9,11},{10,... | collective-permute-start | bytes 393224 | tf_op jit(solution)/shard_map/ppermute | solution.py:46
  43.8 5.0 %collective-permute-start.28 = (bf16[32,2048]{1,0:T(8,128)(2,1)S(1)}, bf16[32,2048]{1,0:T(8,128)(2,1)S(1)}, u32[]{:S(2)}, u32[]{:S(2)}) collective-permute-start(bf16[32,2048]{1,0:T(8,128)(2,1)S(1)} %collective-permute-done.27), channel_id=1, source_target_pairs={{0,8},{1,17},{2,10},{3,19},{4,12},{5,21},{6,14},{7,23},{8,0},{9,25... | collective-permute-start | bytes 393224 | tf_op jit(solution)/shard_map/ppermute | solution.py:56
  45.7 5.0 %collective-permute-start.22 = (bf16[32,2048]{1,0:T(8,128)(2,1)S(1)}, bf16[32,2048]{1,0:T(8,128)(2,1)S(1)}, u32[]{:S(2)}, u32[]{:S(2)}) collective-permute-start(bf16[32,2048]{1,0:T(8,128)(2,1)S(1)} %collective-permute-done.21), channel_id=1, source_target_pairs={{0,8},{1,17},{2,10},{3,19},{4,12},{5,21},{6,14},{7,23},{8,0},{9,25... | collective-permute-start | bytes 393224 | tf_op jit(solution)/shard_map/ppermute | solution.py:56
  48.7 6.3 %collective-permute-start.16 = (bf16[32,2048]{1,0:T(8,128)(2,1)S(1)}, bf16[32,2048]{1,0:T(8,128)(2,1)S(1)}, u32[]{:S(2)}, u32[]{:S(2)}) collective-permute-start(bf16[32,2048]{1,0:T(8,128)(2,1)S(1)} %collective-permute-done.15), channel_id=1, source_target_pairs={{0,8},{1,17},{2,10},{3,19},{4,12},{5,21},{6,14},{7,23},{8,0},{9,25... | collective-permute-start | bytes 393224 | tf_op jit(solution)/shard_map/ppermute | solution.py:56
  50.6 11.3 %collective-permute-start.29 = (bf16[64,2048]{1,0:T(8,128)(2,1)S(1)}, bf16[64,2048]{1,0:T(8,128)(2,1)S(1)}, u32[]{:S(2)}, u32[]{:S(2)}) collective-permute-start(bf16[64,2048]{1,0:T(8,128)(2,1)S(1)} %constant_dynamic-update-slice_fusion.6.refs_0_), channel_id=1, source_target_pairs={{0,16},{1,9},{2,18},{3,11},{4,20},{5,13},{6,22},{7,15},{8,24},{9,1... | collective-permute-start | bytes 786440 | tf_op jit(solution)/shard_map/ppermute | solution.py:56
  55.0 6.4 %collective-permute-start.8 = (bf16[32,2048]{1,0:T(8,128)(2,1)S(1)}, bf16[32,2048]{1,0:T(8,128)(2,1)S(1)}, u32[]{:S(2)}, u32[]{:S(2)}) collective-permute-start(bf16[32,2048]{1,0:T(8,128)(2,1)S(1)} %get-tuple-element.69), channel_id=1, source_target_pairs={{0,8},{1,17},{2,10},{3,19},{4,12},{5,21},{6,14},{7,23},{8,0},{9,25... | collective-permute-start | bytes 393224 | tf_op jit(solution)/shard_map/ppermute | solution.py:56
  61.4 7.4 %collective-permute-start.23 = (bf16[64,2048]{1,0:T(8,128)(2,1)S(1)}, bf16[64,2048]{1,0:T(8,128)(2,1)S(1)}, u32[]{:S(2)}, u32[]{:S(2)}) collective-permute-start(bf16[64,2048]{1,0:T(8,128)(2,1)S(1)} %constant_dynamic-update-slice_fusion.4.refs_0_), channel_id=1, source_target_pairs={{0,16},{1,9},{2,18},{3,11},{4,20},{5,13},{6,22},{7,15},{8,24},{9,1... | collective-permute-start | bytes 786440 | tf_op jit(solution)/shard_map/ppermute | solution.py:56
  61.9 10.5 %collective-permute-start.17 = (bf16[64,2048]{1,0:T(8,128)(2,1)S(1)}, bf16[64,2048]{1,0:T(8,128)(2,1)S(1)}, u32[]{:S(2)}, u32[]{:S(2)}) collective-permute-start(bf16[64,2048]{1,0:T(8,128)(2,1)S(1)} %constant_dynamic-update-slice_fusion.2.refs_0_), channel_id=1, source_target_pairs={{0,16},{1,9},{2,18},{3,11},{4,20},{5,13},{6,22},{7,15},{8,24},{9,1... | collective-permute-start | bytes 786440 | tf_op jit(solution)/shard_map/ppermute | solution.py:56
  63.4 13.6 %collective-permute-start.9 = (bf16[64,2048]{1,0:T(8,128)(2,1)S(1)}, bf16[64,2048]{1,0:T(8,128)(2,1)S(1)}, u32[]{:S(2)}, u32[]{:S(2)}) collective-permute-start(bf16[64,2048]{1,0:T(8,128)(2,1)S(1)} %constant_dynamic-update-slice_fusion.refs_0_), channel_id=1, source_target_pairs={{0,16},{1,9},{2,18},{3,11},{4,20},{5,13},{6,22},{7,15},{8,24},{9,1... | collective-permute-start | bytes 786440 | tf_op jit(solution)/shard_map/ppermute | solution.py:56
  67.2 13.4 %collective-permute-start.30 = (bf16[64,2048]{1,0:T(8,128)(2,1)S(1)}, bf16[64,2048]{1,0:T(8,128)(2,1)S(1)}, u32[]{:S(2)}, u32[]{:S(2)}) collective-permute-start(bf16[64,2048]{1,0:T(8,128)(2,1)S(1)} %get-tuple-element.80), channel_id=1, source_target_pairs={{0,16},{1,9},{2,18},{3,11},{4,20},{5,13},{6,22},{7,15},{8,24},{9,1... | collective-permute-start | bytes 786440 | tf_op jit(solution)/shard_map/ppermute | solution.py:56
  71.8 10.7 %collective-permute-start.24 = (bf16[64,2048]{1,0:T(8,128)(2,1)S(1)}, bf16[64,2048]{1,0:T(8,128)(2,1)S(1)}, u32[]{:S(2)}, u32[]{:S(2)}) collective-permute-start(bf16[64,2048]{1,0:T(8,128)(2,1)S(1)} %get-tuple-element.78), channel_id=1, source_target_pairs={{0,16},{1,9},{2,18},{3,11},{4,20},{5,13},{6,22},{7,15},{8,24},{9,1... | collective-permute-start | bytes 786440 | tf_op jit(solution)/shard_map/ppermute | solution.py:56
  75.4 12.0 %collective-permute-start.18 = (bf16[64,2048]{1,0:T(8,128)(2,1)S(1)}, bf16[64,2048]{1,0:T(8,128)(2,1)S(1)}, u32[]{:S(2)}, u32[]{:S(2)}) collective-permute-start(bf16[64,2048]{1,0:T(8,128)(2,1)S(1)} %get-tuple-element.76), channel_id=1, source_target_pairs={{0,16},{1,9},{2,18},{3,11},{4,20},{5,13},{6,22},{7,15},{8,24},{9,1... | collective-permute-start | bytes 786440 | tf_op jit(solution)/shard_map/ppermute | solution.py:56
  80.0 10.2 %collective-permute-start.13 = (bf16[64,2048]{1,0:T(8,128)(2,1)S(1)}, bf16[64,2048]{1,0:T(8,128)(2,1)S(1)}, u32[]{:S(2)}, u32[]{:S(2)}) collective-permute-start(bf16[64,2048]{1,0:T(8,128)(2,1)S(1)} %get-tuple-element.74), channel_id=1, source_target_pairs={{0,16},{1,9},{2,18},{3,11},{4,20},{5,13},{6,22},{7,15},{8,24},{9,1... | collective-permute-start | bytes 786440 | tf_op jit(solution)/shard_map/ppermute | solution.py:56
  80.6 10.2 %collective-permute-start.31 = (bf16[32,2048]{1,0:T(8,128)(2,1)S(1)}, bf16[32,2048]{1,0:T(8,128)(2,1)S(1)}, u32[]{:S(2)}, u32[]{:S(2)}) collective-permute-start(bf16[32,2048]{1,0:T(8,128)(2,1)S(1)} %add_convert_fusion.2), channel_id=1, source_target_pairs={{0,8},{1,17},{2,10},{3,19},{4,12},{5,21},{6,14},{7,23},{8,0},{9,25... | collective-permute-start | bytes 393224 | tf_op jit(solution)/shard_map/ppermute | solution.py:56
  82.6 9.6 %collective-permute-start.25 = (bf16[32,2048]{1,0:T(8,128)(2,1)S(1)}, bf16[32,2048]{1,0:T(8,128)(2,1)S(1)}, u32[]{:S(2)}, u32[]{:S(2)}) collective-permute-start(bf16[32,2048]{1,0:T(8,128)(2,1)S(1)} %add_convert_fusion.4), channel_id=1, source_target_pairs={{0,8},{1,17},{2,10},{3,19},{4,12},{5,21},{6,14},{7,23},{8,0},{9,25... | collective-permute-start | bytes 393224 | tf_op jit(solution)/shard_map/ppermute | solution.py:56
  87.5 5.5 %collective-permute-start.19 = (bf16[32,2048]{1,0:T(8,128)(2,1)S(1)}, bf16[32,2048]{1,0:T(8,128)(2,1)S(1)}, u32[]{:S(2)}, u32[]{:S(2)}) collective-permute-start(bf16[32,2048]{1,0:T(8,128)(2,1)S(1)} %add_convert_fusion.6), channel_id=1, source_target_pairs={{0,8},{1,17},{2,10},{3,19},{4,12},{5,21},{6,14},{7,23},{8,0},{9,25... | collective-permute-start | bytes 393224 | tf_op jit(solution)/shard_map/ppermute | solution.py:56
  90.3 5.3 %collective-permute-start.14 = (bf16[32,2048]{1,0:T(8,128)(2,1)S(1)}, bf16[32,2048]{1,0:T(8,128)(2,1)S(1)}, u32[]{:S(2)}, u32[]{:S(2)}) collective-permute-start(bf16[32,2048]{1,0:T(8,128)(2,1)S(1)} %add_convert_fusion.8), channel_id=1, source_target_pairs={{0,8},{1,17},{2,10},{3,19},{4,12},{5,21},{6,14},{7,23},{8,0},{9,25... | collective-permute-start | bytes 393224 | tf_op jit(solution)/shard_map/ppermute | solution.py:56
  90.9 7.0 %collective-permute-start.32 = (bf16[32,2048]{1,0:T(8,128)(2,1)S(1)}, bf16[32,2048]{1,0:T(8,128)(2,1)S(1)}, u32[]{:S(2)}, u32[]{:S(2)}) collective-permute-start(bf16[32,2048]{1,0:T(8,128)(2,1)S(1)} %add_convert_fusion.1), channel_id=1, source_target_pairs={{0,6},{1,7},{2,4},{3,5},{4,2},{5,3},{6,0},{7,1},{8,14},{9,15},{10,... | collective-permute-start | bytes 393224 | tf_op jit(solution)/shard_map/ppermute | solution.py:46
  92.3 8.3 %collective-permute-start.26 = (bf16[32,2048]{1,0:T(8,128)(2,1)S(1)}, bf16[32,2048]{1,0:T(8,128)(2,1)S(1)}, u32[]{:S(2)}, u32[]{:S(2)}) collective-permute-start(bf16[32,2048]{1,0:T(8,128)(2,1)S(1)} %add_convert_fusion.3), channel_id=1, source_target_pairs={{0,4},{1,5},{2,6},{3,7},{4,0},{5,1},{6,2},{7,3},{8,12},{9,13},{10,... | collective-permute-start | bytes 393224 | tf_op jit(solution)/shard_map/ppermute | solution.py:46
  93.0 7.6 %collective-permute-start.20 = (bf16[32,2048]{1,0:T(8,128)(2,1)S(1)}, bf16[32,2048]{1,0:T(8,128)(2,1)S(1)}, u32[]{:S(2)}, u32[]{:S(2)}) collective-permute-start(bf16[32,2048]{1,0:T(8,128)(2,1)S(1)} %add_convert_fusion.5), channel_id=1, source_target_pairs={{0,2},{1,3},{2,0},{3,1},{4,6},{5,7},{6,4},{7,5},{8,10},{9,11},{10,... | collective-permute-start | bytes 393224 | tf_op jit(solution)/shard_map/ppermute | solution.py:46
